TPU v7x, 256 devices: a whole 4x4x8 slice. The times are simulated.
256 devices in a mesh: sp: 32 (over z, y), tp: 8 (over x, core).
Axes of the slice: x: 4, y: 4, z: 8, core: 2. Of those that a mesh axis runs over, the one named last changes fastest.
Arguments:
- tokens: bfloat16 [16384, 2048], P('sp', 'tp'), may hold values from -400 to 400
- norm_gain: float32 [2048], replicated, may hold values from 0.1 to 1.9
- query_weight: bfloat16 [2048, 1024], P(None, 'tp'), may hold values from -0.37306796 to 0.37306796
- key_weight: bfloat16 [2048, 1024], P(None, 'tp'), may hold values from -0.2625825 to 0.2625825
- value_weight: bfloat16 [2048, 1024], P(None, 'tp'), may hold values from -0.125 to 0.125
- outer_gate_weight: bfloat16 [2048, 1024], P(None, 'tp'), may hold values from -0.125 to 0.125
- inner_gate_weight: bfloat16 [2048, 1024], P(None, 'tp'), may hold values from -0.125 to 0.125
- conv_input_weight: bfloat16 [2048, 1024], P(None, 'tp'), may hold values from -0.125 to 0.125
- conv_taps: float32 [3, 1024], P(None, 'tp'), may hold values from -3.5 to 3.5
- lambdas: float32 [8], P('tp'), may hold values from 0.3 to 0.8
- head_gain: float32 [128], replicated, may hold values from 0.1 to 1.9
- attn_out_weight: bfloat16 [1024, 2048], P(None, 'tp'), may hold values from -0.125 to 0.125
- conv_out_weight: bfloat16 [1024, 2048], P(None, 'tp'), may hold values from -0.125 to 0.125
Outputs:
- mixed_out: bfloat16 [16384, 2048], P('sp', 'tp')
- log_totals: float32 [8, 2, 16384], P('tp', None, 'sp')
All inputs are finite; a program needn't handle non-finite values.
Results may differ from a plain program's by a relative error of at most 0.014.
The roundings to bfloat16 on the way count: a program that leaves them out, or rounds other values in their place, can miss the bound.
Values may be sent and summed in bfloat16 or wider, within the bound.
A program may use at most 128 MiB of HBM per device.

v0:
```python
import math

import jax
import jax.numpy as jnp
from jax import lax
from jax.sharding import PartitionSpec as P

NORM_EPS = 1e-06
HEAD_EPS = 1e-05
ROPE_BASE = 500000.0
MASKED = -1e30
HEAD_SCALE = 0.8


def joined_along(pieces, dim):
    pieces = jnp.moveaxis(pieces, 0, dim)
    lengths = pieces.shape
    return pieces.reshape(*lengths[:dim], lengths[dim] * lengths[dim + 1], *lengths[dim + 2 :])


def from_everyone(x, axis):
    peers = lax.axis_size(axis)
    return lax.all_to_all(jnp.broadcast_to(x[None], (peers, *x.shape)), axis, 0, 0, tiled=True)


def gather_directly(x, axis, dim):
    return joined_along(from_everyone(x, axis), dim)


def shifted(block, axis, distance):
    devices = range(lax.axis_size(axis))
    route = [(i - distance, i) for i in devices if i - distance in devices]
    return lax.ppermute(block, axis, route)


def side_by_side(arrays, axis, dim, along):
    columns = [a.reshape(*a.shape[:along], -1) for a in arrays]
    both = jnp.concatenate(columns, axis=along)
    out, at, outs = (lax.all_gather(both, axis, axis=dim, tiled=True), 0, [])
    for a, column in zip(arrays, columns):
        section = out[..., at : at + column.shape[along]]
        outs.append(section.reshape(*section.shape[:along], *a.shape[along:]))
        at += column.shape[along]
    return tuple(outs)


def side_by_side_2(arrays, axis, dim, along):
    both = jnp.concatenate(arrays, axis=along)
    out, at, outs = (lax.all_gather(both, axis, axis=dim, tiled=True), 0, [])
    for a in arrays:
        outs.append(lax.slice_in_dim(out, at, at + a.shape[along], axis=along))
        at += a.shape[along]
    return tuple(outs)


def rotate(field_in, positions):
    half_dim = field_in.shape[-1] // 2
    frequency = ROPE_BASE ** (-jnp.arange(half_dim, dtype=jnp.float32) * 2.0 / field_in.shape[-1])
    angles = positions[:, None] * frequency[None, :]
    cosine = jnp.cos(angles)[:, None, None, :]
    sine_part = jnp.sin(angles)[:, None, None, :]
    first_half = field_in[..., :half_dim]
    second_half = field_in[..., half_dim:]
    return jnp.concatenate(
        [
            first_half * cosine - second_half * sine_part,
            second_half * cosine + first_half * sine_part,
        ],
        axis=-1,
    )


def add_products(block_in, norm_gain, weights):
    floats = block_in.astype(jnp.float32)
    scaled = (floats * norm_gain[None, :]).astype(jnp.bfloat16)
    products = tuple(
        (jnp.dot(scaled, weight, preferred_element_type=jnp.float32) for weight in weights)
    )
    return (jnp.sum(floats * floats, axis=1, keepdims=True),) + products


def over_shards(step_fn, running, arrays, anchor, local_rows):
    shard_count = arrays[0].shape[0] // local_rows
    group_size = math.gcd(shard_count, max(1, 2048 // local_rows))
    block_rows = group_size * local_rows
    steps_count = shard_count // group_size
    stacked = tuple(
        (member.reshape((steps_count, block_rows) + member.shape[1:]) for member in arrays)
    )

    def scan_step(carried, scan_items):
        members, step_index = scan_items
        return (step_fn(carried, members, anchor + step_index * block_rows), None)

    result, unused = lax.scan(
        scan_step, running, (stacked, jnp.arange(steps_count, dtype=jnp.int32))
    )
    return result


def per_device(
    tokens,
    norm_gain,
    query_weight,
    key_weight,
    value_weight,
    outer_gate_weight,
    inner_gate_weight,
    conv_input_weight,
    conv_taps,
    lambdas,
    head_gain,
    attn_out_weight,
    conv_out_weight,
):
    local_rows = tokens.shape[0]
    local_heads = lambdas.shape[0]
    head_dim = query_weight.shape[1] // (2 * local_heads)
    value_dim = 2 * head_dim
    taps_count = conv_taps.shape[0]
    width_all = norm_gain.shape[0]
    columns_dev = query_weight.shape[1]
    attn_weights = (query_weight, key_weight, value_weight)
    conv_weights = (outer_gate_weight, inner_gate_weight, conv_input_weight)
    squares, query_raw, key_raw, value_raw, outer_raw, inner_raw, signal_raw = add_products(
        gather_directly(tokens, "tp", 1), norm_gain, attn_weights + conv_weights
    )
    inverse_rms = lax.rsqrt(squares / width_all + NORM_EPS)
    query_pos = lax.axis_index("sp") * local_rows + jnp.arange(local_rows, dtype=jnp.int32)
    positions = query_pos.astype(jnp.float32)
    queries = rotate(
        (inverse_rms * query_raw).reshape(local_rows, local_heads, 2, head_dim), positions
    ).astype(jnp.bfloat16)
    key_rows = rotate(
        (inverse_rms * key_raw).reshape(local_rows, local_heads, 2, head_dim), positions
    ).astype(jnp.bfloat16)
    values = (
        (inverse_rms * value_raw).astype(jnp.bfloat16).reshape(local_rows, local_heads, value_dim)
    )
    outer_gate = (inverse_rms * outer_raw).astype(jnp.bfloat16)
    inner_gate = (inverse_rms * inner_raw).astype(jnp.bfloat16)
    signal = (inverse_rms * signal_raw).astype(jnp.bfloat16)
    conv_in = (inner_gate.astype(jnp.float32) * signal.astype(jnp.float32)).astype(jnp.bfloat16)
    rim_rows = shifted(conv_in[local_rows - (taps_count - 1) :], "sp", 1)
    padded = jnp.concatenate([rim_rows, conv_in], axis=0)
    summed = jnp.zeros((local_rows, columns_dev), jnp.float32)
    for tap_index in range(taps_count):
        summed = summed + conv_taps[tap_index][None, :] * padded[
            tap_index : tap_index + local_rows
        ].astype(jnp.float32)
    conv_out = (outer_gate.astype(jnp.float32) * summed).astype(jnp.bfloat16)
    scale_factor = head_dim ** (-0.5)

    def block_scores(key_block, key_anchor):
        scores = (
            jnp.einsum("qhcd,khcd->hcqk", queries, key_block, preferred_element_type=jnp.float32)
            * scale_factor
        )
        visible = (
            query_pos[:, None]
            >= (key_anchor + jnp.arange(key_block.shape[0], dtype=jnp.int32))[None, :]
        )
        return (jnp.where(visible, scores, MASKED), visible)

    def stats_step(running, members, key_anchor):
        max_before, sum_before = running
        scores, visible = block_scores(members[0], key_anchor)
        max_after = jnp.maximum(max_before, jnp.max(scores, axis=-1))
        exponent = jnp.where(visible, jnp.exp(scores - max_after[..., None]), 0.0)
        return (
            max_after,
            sum_before * jnp.exp(max_before - max_after) + jnp.sum(exponent, axis=-1),
        )

    stats_init = (
        jnp.full((local_heads, 2, local_rows), MASKED, jnp.float32),
        jnp.zeros((local_heads, 2, local_rows), jnp.float32),
    )
    value_init = jnp.zeros((local_rows, local_heads, value_dim), jnp.float32)

    def value_step_with(row_max, row_sum):

        def value_step(running, members, key_anchor):
            scores, visible = block_scores(members[0], key_anchor)
            normalized = jnp.where(
                visible, jnp.exp(scores - row_max[..., None]) / row_sum[..., None], 0.0
            )
            weights = (normalized[:, 0] - lambdas[:, None, None] * normalized[:, 1]).astype(
                jnp.bfloat16
            )
            return running + jnp.einsum(
                "hqk,khv->qhv", weights, members[1], preferred_element_type=jnp.float32
            )

        return value_step

    all_keys, all_values = side_by_side((key_rows, values), "sp", 0, 2)
    row_max, row_sum = over_shards(stats_step, stats_init, (all_keys,), 0, local_rows)
    head_mix = over_shards(
        value_step_with(row_max, row_sum), value_init, (all_keys, all_values), 0, local_rows
    )
    log_totals = row_max + jnp.log(row_sum)
    normed = (
        head_mix
        * lax.rsqrt(jnp.mean(head_mix * head_mix, axis=-1, keepdims=True) + HEAD_EPS)
        * head_gain[None, None, :]
        * HEAD_SCALE
    )
    attn_out = normed.astype(jnp.bfloat16).reshape(local_rows, local_heads * value_dim)
    running = jnp.zeros((local_rows, attn_out_weight.shape[1]), jnp.float32)
    pieces = side_by_side_2((attn_out, conv_out), "tp", 1, 0)
    running = jnp.dot(pieces[0], attn_out_weight, preferred_element_type=jnp.float32)
    mixed_out = running + jnp.dot(pieces[1], conv_out_weight, preferred_element_type=jnp.float32)
    return (mixed_out.astype(jnp.bfloat16), log_totals)


def solution(mesh):
    in_specs = (
        P("sp", "tp"),
        P(),
        P(None, "tp"),
        P(None, "tp"),
        P(None, "tp"),
        P(None, "tp"),
        P(None, "tp"),
        P(None, "tp"),
        P(None, "tp"),
        P("tp"),
        P(),
        P(None, "tp"),
        P(None, "tp"),
    )
    out_specs = (P("sp", "tp"), P("tp", None, "sp"))
    return jax.shard_map(
        per_device, mesh=mesh, in_specs=in_specs, out_specs=out_specs, check_vma=False
    )
```

profile of v0, /device:TPU:225, one launch (start us, length us, event | category | flops | bytes accessed | tf_op | source)
XLA Modules:
  0.0 332.9 jit_solution(14198621548347067425)
XLA Ops:
  9.9 5.0 %all-to-all-start = ((bf16[8,512,256]{1,2,0:T(8,128)(2,1)}), bf16[8,512,256]{1,2,0:T(8,128)(2,1)S(1)}, u32[]{:S(2)}, u32[]{:S(2)}) async-start(bf16[8,512,256]{1,2,0:T(8,128)(2,1)} %broadcast_in_dim.58), calls=%async_computation | async-start | bytes 4194304 | tf_op jit(solution)/shard_map/all_to_all | solution.py:23
  15.2 25.9 %all-to-all-done = bf16[8,512,256]{1,2,0:T(8,128)(2,1)S(1)} async-done(((bf16[8,512,256]{1,2,0:T(8,128)(2,1)}), bf16[8,512,256]{1,2,0:T(8,128)(2,1)S(1)}, u32[]{:S(2)}, u32[]{:S(2)}) %all-to-all-start) | async-done | bytes 2097184 | tf_op jit(solution)/shard_map/all_to_all | solution.py:23
  49.8 3.2 collective-permute-start
  53.0 3.5 %collective-permute-done = bf16[2,128]{0,1:T(8,128)(2,1)S(1)} collective-permute-done((bf16[2,128]{0,1:T(8,128)(2,1)S(1)}, bf16[2,128]{0,1:T(8,128)(2,1)S(1)}, u32[]{:S(2)}, u32[]{:S(2)}) %collective-permute-start) | collective-permute-done | bytes 544 | tf_op jit(solution)/shard_map/ppermute | solution.py:33
  58.1 84.1 %all-gather.3.cloned.1.call-done = bf16[16384,1,256]{0,2,1:T(8,128)(2,1)} async-done(((bf16[512,1,256]{0,2,1:T(8,128)(2,1)}), bf16[16384,1,256]{0,2,1:T(8,128)(2,1)}) %all-gather.3.cloned.1.call-update) | async-done | bytes 8388624 | tf_op jit(solution)/shard_map/all_gather | solution.py:39
  142.3 5.1 %fusion.52 = (bf16[16384,1,128]{0,2,1:T(8,128)(2,1)S(1)}, bf16[16384,1,128]{0,2,1:T(8,128)(2,1)}) fusion(bf16[16384,1,256]{0,2,1:T(8,128)(2,1)} %all-gather.3.cloned.1.call-done), kind=kLoop, calls=%fused_computation.91 | loop fusion | bytes 16777216 | tf_op jit(solution)/shard_map/slice | solution.py:41
  147.3 3.2 copy.32
  150.5 4.2 %copy.24 = bf16[8,2048,1,2,64]{1,4,3,2,0:T(8,128)(2,1)} copy(bf16[8,2048,1,2,64]{1,0,4,3,2:T(8,128)(2,1)S(1)} %bitcast.140) | data formatting | bytes 8388608
  154.8 58.8 %while.24 = (s32[]{:T(128)}, f32[1,2,512]{2,1,0:T(2,128)S(1)}, f32[1,2,512]{2,1,0:T(2,128)S(1)}, s32[8]{0:T(128)S(1)}, bf16[8,2048,1,2,64]{1,4,3,2,0:T(8,128)(2,...) while((s32[]{:T(128)}, f32[1,2,512]{2,1,0:T(2,128)S(1)}, ...), condition=%wide.region_4.5_spmd.clone, body=%wide.region_1.4_spmd.clone.sunk | while | flops 286268928 | bytes 20652188 | solution.py:95
  156.8 3.0 fusion.74
  164.2 3.0 fusion.74
  171.5 3.0 fusion.74
  178.9 3.0 fusion.74
  186.2 3.0 fusion.74
  193.6 3.0 fusion.74
  200.9 3.0 fusion.74
  208.3 3.0 fusion.74
  213.6 6.4 %copy.31 = bf16[16384,1,128]{2,0,1:T(8,128)(2,1)} copy(bf16[16384,1,128]{0,2,1:T(8,128)(2,1)} %get-tuple-element.229) | data formatting | bytes 8388608
  220.0 68.8 %while.25 = (s32[]{:T(128)}, f32[512,1,128]{0,2,1:T(8,128)S(1)}, bf16[8,2048,1,128]{3,1,2,0:T(8,128)(2,1)}, s32[8]{0:T(128)S(1)}, bf16[8,2048,1,2,64]{1,4,3,2,0:...) while((s32[]{:T(128)}, f32[512,1,128]{0,2,1:T(8,128)S(1)}, ...), condition=%wide.region_6.7_spmd.clone, body=%wide.region_5.6_spmd.clone.sunk | while | flops 551684608 | bytes 20607672 | solution.py:95
  222.1 4.2 %fusion.79 = f32[1,2,512,2048]{2,3,1,0:T(8,128)S(1)} fusion(f32[2,512]{1,0:T(2,128)S(1)} %bitcast.148, f32[2,512]{1,0:T(2,128)S(1)} %bitcast.145, pred[512,2048]{0,1:T(8,128)(4,1)S(1)} %broadcast_compare_fusion.5, bf16[8,2048,1,2,64]{1,4,3,2,0:T(8,128)(2,1)} %get-tuple-element.411, s32[]{:T(128)S(6)} %copy.44, ...), kind=kOutput, calls=%fused_computation.22.clone.1 | convolution fusion | flops 278921216 | bytes 10100740 | tf_op jit(solution)/shard_map/while/body/eval_jaxpr/qhcd,khcd->hcqk/dot_general | solution.py:156
  226.2 2.4 fusion.80
  230.7 4.2 %fusion.79 = f32[1,2,512,2048]{2,3,1,0:T(8,128)S(1)} fusion(f32[2,512]{1,0:T(2,128)S(1)} %bitcast.148, f32[2,512]{1,0:T(2,128)S(1)} %bitcast.145, pred[512,2048]{0,1:T(8,128)(4,1)S(1)} %broadcast_compare_fusion.5, bf16[8,2048,1,2,64]{1,4,3,2,0:T(8,128)(2,1)} %get-tuple-element.411, s32[]{:T(128)S(6)} %copy.44, ...), kind=kOutput, calls=%fused_computation.22.clone.1 | convolution fusion | flops 278921216 | bytes 10100740 | tf_op jit(solution)/shard_map/while/body/eval_jaxpr/qhcd,khcd->hcqk/dot_general | solution.py:156
  234.8 2.4 fusion.80
  239.3 4.2 %fusion.79 = f32[1,2,512,2048]{2,3,1,0:T(8,128)S(1)} fusion(f32[2,512]{1,0:T(2,128)S(1)} %bitcast.148, f32[2,512]{1,0:T(2,128)S(1)} %bitcast.145, pred[512,2048]{0,1:T(8,128)(4,1)S(1)} %broadcast_compare_fusion.5, bf16[8,2048,1,2,64]{1,4,3,2,0:T(8,128)(2,1)} %get-tuple-element.411, s32[]{:T(128)S(6)} %copy.44, ...), kind=kOutput, calls=%fused_computation.22.clone.1 | convolution fusion | flops 278921216 | bytes 10100740 | tf_op jit(solution)/shard_map/while/body/eval_jaxpr/qhcd,khcd->hcqk/dot_general | solution.py:156
  247.9 4.2 %fusion.79 = f32[1,2,512,2048]{2,3,1,0:T(8,128)S(1)} fusion(f32[2,512]{1,0:T(2,128)S(1)} %bitcast.148, f32[2,512]{1,0:T(2,128)S(1)} %bitcast.145, pred[512,2048]{0,1:T(8,128)(4,1)S(1)} %broadcast_compare_fusion.5, bf16[8,2048,1,2,64]{1,4,3,2,0:T(8,128)(2,1)} %get-tuple-element.411, s32[]{:T(128)S(6)} %copy.44, ...), kind=kOutput, calls=%fused_computation.22.clone.1 | convolution fusion | flops 278921216 | bytes 10100740 | tf_op jit(solution)/shard_map/while/body/eval_jaxpr/qhcd,khcd->hcqk/dot_general | solution.py:156
  252.1 2.4 fusion.80
  256.5 4.2 %fusion.79 = f32[1,2,512,2048]{2,3,1,0:T(8,128)S(1)} fusion(f32[2,512]{1,0:T(2,128)S(1)} %bitcast.148, f32[2,512]{1,0:T(2,128)S(1)} %bitcast.145, pred[512,2048]{0,1:T(8,128)(4,1)S(1)} %broadcast_compare_fusion.5, bf16[8,2048,1,2,64]{1,4,3,2,0:T(8,128)(2,1)} %get-tuple-element.411, s32[]{:T(128)S(6)} %copy.44, ...), kind=kOutput, calls=%fused_computation.22.clone.1 | convolution fusion | flops 278921216 | bytes 10100740 | tf_op jit(solution)/shard_map/while/body/eval_jaxpr/qhcd,khcd->hcqk/dot_general | solution.py:156
  265.1 4.2 %fusion.79 = f32[1,2,512,2048]{2,3,1,0:T(8,128)S(1)} fusion(f32[2,512]{1,0:T(2,128)S(1)} %bitcast.148, f32[2,512]{1,0:T(2,128)S(1)} %bitcast.145, pred[512,2048]{0,1:T(8,128)(4,1)S(1)} %broadcast_compare_fusion.5, bf16[8,2048,1,2,64]{1,4,3,2,0:T(8,128)(2,1)} %get-tuple-element.411, s32[]{:T(128)S(6)} %copy.44, ...), kind=kOutput, calls=%fused_computation.22.clone.1 | convolution fusion | flops 278921216 | bytes 10100740 | tf_op jit(solution)/shard_map/while/body/eval_jaxpr/qhcd,khcd->hcqk/dot_general | solution.py:156
  273.7 4.2 %fusion.79 = f32[1,2,512,2048]{2,3,1,0:T(8,128)S(1)} fusion(f32[2,512]{1,0:T(2,128)S(1)} %bitcast.148, f32[2,512]{1,0:T(2,128)S(1)} %bitcast.145, pred[512,2048]{0,1:T(8,128)(4,1)S(1)} %broadcast_compare_fusion.5, bf16[8,2048,1,2,64]{1,4,3,2,0:T(8,128)(2,1)} %get-tuple-element.411, s32[]{:T(128)S(6)} %copy.44, ...), kind=kOutput, calls=%fused_computation.22.clone.1 | convolution fusion | flops 278921216 | bytes 10100740 | tf_op jit(solution)/shard_map/while/body/eval_jaxpr/qhcd,khcd->hcqk/dot_general | solution.py:156
  282.3 4.2 %fusion.79 = f32[1,2,512,2048]{2,3,1,0:T(8,128)S(1)} fusion(f32[2,512]{1,0:T(2,128)S(1)} %bitcast.148, f32[2,512]{1,0:T(2,128)S(1)} %bitcast.145, pred[512,2048]{0,1:T(8,128)(4,1)S(1)} %broadcast_compare_fusion.5, bf16[8,2048,1,2,64]{1,4,3,2,0:T(8,128)(2,1)} %get-tuple-element.411, s32[]{:T(128)S(6)} %copy.44, ...), kind=kOutput, calls=%fused_computation.22.clone.1 | convolution fusion | flops 278921216 | bytes 10100740 | tf_op jit(solution)/shard_map/while/body/eval_jaxpr/qhcd,khcd->hcqk/dot_general | solution.py:156
  290.4 31.5 %all-gather.5.cloned.1.call-done = bf16[1024,1024]{0,1:T(8,128)(2,1)} async-done(((bf16[1024,128]{0,1:T(8,128)(2,1)}), bf16[1024,1024]{0,1:T(8,128)(2,1)}) %all-gather.5.cloned.1.call-update) | async-done | bytes 2097168 | tf_op jit(solution)/shard_map/all_gather | solution.py:49
  323.7 2.4 fusion.34
  (153 shorter events, 68.2 us)
Async XLA Ops:
  7.2 314.8 %copy-start = (bf16[1024,256]{1,0:T(8,128)(2,1)S(1)}, bf16[1024,256]{1,0:T(8,128)(2,1)}, u32[]{:S(2)}) copy-start(bf16[1024,256]{1,0:T(8,128)(2,1)} %param.28) | copy-start | bytes 1572868
  8.3 33.2 %copy-start.3 = (f32[2048]{0:T(1024)S(1)}, f32[2048]{0:T(1024)}, u32[]{:S(2)}) copy-start(f32[2048]{0:T(1024)} %param.18) | copy-start | bytes 24580
  9.9 31.2 %all-to-all-start = ((bf16[8,512,256]{1,2,0:T(8,128)(2,1)}), bf16[8,512,256]{1,2,0:T(8,128)(2,1)S(1)}, u32[]{:S(2)}, u32[]{:S(2)}) async-start(bf16[8,512,256]{1,2,0:T(8,128)(2,1)} %broadcast_in_dim.58), calls=%async_computation | async-start | bytes 4194304 | tf_op jit(solution)/shard_map/all_to_all | solution.py:23
  14.8 127.4 %all-gather.3.cloned.1.call-start = ((), (), s32[]{:S(2)}) async-start(), calls=%async_computation.1 | async-start | bytes 8650752 | tf_op jit(solution)/shard_map/all_gather | solution.py:39
  41.0 3.0 copy-start.6
  41.6 2.9 copy-start.7
  42.0 3.0 copy-start.1
  45.0 3.1 copy-start.2
  45.1 7.8 %copy-start.4 = (f32[3,128]{1,0:T(4,128)S(1)}, f32[3,128]{1,0:T(4,128)}, u32[]{:S(2)}) copy-start(f32[3,128]{1,0:T(4,128)} %param.25) | copy-start | bytes 4612
  45.9 276.0 %all-gather.5.cloned.1.call-start = ((), (), s32[]{:S(2)}) async-start(), calls=%async_computation.2 | async-start | bytes 2359296 | tf_op jit(solution)/shard_map/all_gather | solution.py:49
  49.8 6.8 %collective-permute-start = (bf16[2,128]{0,1:T(8,128)(2,1)S(1)}, bf16[2,128]{0,1:T(8,128)(2,1)S(1)}, u32[]{:S(2)}, u32[]{:S(2)}) collective-permute-start(bf16[2,128]{0,1:T(8,128)(2,1)S(1)} %slice.72), channel_id=1, source_target_pairs={{0,8},{8,16},{16,24},{24,32},{32,40},{40,48},{48,56},{56,64},{64,7... | collective-permute-start | bytes 1544 | tf_op jit(solution)/shard_map/ppermute | solution.py:33
  220.0 68.9 %copy-start.5 = (f32[128]{0:T(128)S(1)}, f32[128]{0:T(128)}, u32[]{:S(2)}) copy-start(f32[128]{0:T(128)} %param.27) | copy-start | bytes 1540
  288.9 34.8 %copy-start.8 = (bf16[1024,256]{1,0:T(8,128)(2,1)S(1)}, bf16[1024,256]{1,0:T(8,128)(2,1)}, u32[]{:S(2)}) copy-start(bf16[1024,256]{1,0:T(8,128)(2,1)} %param.29) | copy-start | bytes 1572868
Sparse Core Ops, SparseCore 0:
  46.0 96.1 all-gather.2
  289.9 31.9 all-gather.4
where the time goes:
time: 338 us; the launch traced here: 333 us
  waiting for transfers between devices  145 us (43%)
  matrix products  88.6 us (26%)
  other arithmetic  34.2 us (10%)
  local copies, waits for them, and re-layouts  31.1 us (9%)
  between operations  14.3 us (4%)
  loops' own time  11.4 us (3%)
  starting transfers between devices  8.21 us (2%)
    all_gather x1, waiting for transfers between devices, side_by_side(): out, at, outs = (lax.all_gather(both, axis, axis=dim, tiled=True), 0, [])  84.1 us
    dot_general x16, matrix products, block_scores(): jnp.einsum('qhcd,khcd->hcqk', queries, key_block, preferred_element_type=...  57.3 us
    all_gather x1, waiting for transfers between devices, side_by_side_2(): out, at, outs = (lax.all_gather(both, axis, axis=dim, tiled=True), 0, [])  31.5 us
    all_to_all x1, waiting for transfers between devices, from_everyone(): lax.all_to_all(jnp.broadcast_to(x[None], (peers, *x.shape)), axis, 0, 0,...  25.9 us
    dot_general x8, matrix products, value_step(): jnp.einsum('hqk,khv->qhv', weights, members[1], preferred_element_type=jn...  19 us
    reduce_sum x8, other arithmetic, stats_step(): jnp.sum(exponent, axis=-1)  18 us
    unnamed x22, local copies, waits for them, and re-layouts  15.1 us
    ge x16, other arithmetic, block_scores(): query_pos[:, None]  12.2 us
  transfers between devices with their start and end apart: 4, of which 4 were waited for; matrix products, arithmetic and copies ran while one was open for 2% of the time, Pallas kernels for 0%

commit v1 on v0

v1 whole, which is shorter than its diff:
```python
import math

import jax
import jax.numpy as jnp
from jax import lax
from jax.experimental import pallas as pl
from jax.experimental.pallas import tpu as pltpu
from jax.sharding import PartitionSpec as P

NORM_EPS = 1e-06
HEAD_EPS = 1e-05
ROPE_BASE = 500000.0
MASKED = -1e30
HEAD_SCALE = 0.8
MESH = pl.DeviceIdType.MESH

NY, NZ, NX, CORES = 4, 8, 4, 2
NTP = NX * CORES
ROWS = 512
HALF = ROWS // 2
PIECE = 256
DIM = 64
VDIM = 128
TILE = 256
LANES = 2 * TILE
TILES = NY * ROWS // TILE
ONES_ROWS = 16
LOG2E = math.log2(math.e)
LN2 = math.log(2.0)


def f32(x):
    return x.astype(jnp.float32)


def bf16(x):
    return x.astype(jnp.bfloat16)


def remote(src, dst, send_sem, recv_sem, device):
    return pltpu.make_async_remote_copy(
        src_ref=src,
        dst_ref=dst,
        send_sem=send_sem,
        recv_sem=recv_sem,
        device_id=device,
        device_id_type=MESH,
    )


class TpGather:
    def __init__(self, own, buf, send, recv, sp, x, c):
        self.own, self.buf, self.send, self.recv = own, buf, send, recv
        self.slot = lambda dx, other: lax.rem(x + dx + NX, NX) * CORES + (1 - c if other else c)
        self.partner = (sp, x * CORES + 1 - c)
        self.right = (sp, self.slot(1, False))
        self.left = (sp, self.slot(-1, False))
        self.started = 0

    def rows(self, h):
        half = self.buf.shape[1] // 2
        return pl.ds(h * half, half)

    def push(self, dx, h, device, first=False):
        slot = self.slot(dx, False)
        block = self.buf.at[slot, self.rows(h)]
        source = self.own.at[self.rows(h)] if first else block
        remote(source, block, self.send.at[self.started], self.recv.at[slot, h], device).start()
        self.started += 1

    def wait(self, dx, other, h):
        slot = self.slot(dx, other)
        block = self.buf.at[slot, self.rows(h)]
        remote(block, block, self.send.at[0], self.recv.at[slot, h], self.partner).wait_recv()

    def start(self):
        self.push(0, 0, self.right, True)
        self.push(0, 1, self.left, True)
        self.push(0, 1, self.right, True)
        self.push(0, 0, self.left, True)
        self.push(0, 0, self.partner, True)
        self.push(0, 1, self.partner, True)

    def neighbours_first(self):
        self.wait(-1, False, 0)
        self.push(-1, 0, self.right)
        self.push(-1, 0, self.partner)
        self.wait(1, False, 1)
        self.push(1, 1, self.left)
        self.push(1, 1, self.partner)

    def neighbours_second(self):
        self.wait(-1, False, 1)
        self.push(-1, 1, self.partner)
        self.wait(1, False, 0)
        self.push(1, 0, self.partner)

    def opposite(self, h):
        self.wait(2, False, h)
        self.push(2, h, self.partner)

    def finish(self):
        block = self.buf.at[0, self.rows(0)]
        for i in range(self.started):
            remote(block, block, self.send.at[i], self.recv.at[0, 0], self.partner).wait_send()


def kernel(
    tok, gain, wq, wk, wv, wo, wi, ws, cosine, sine, taps, lam, head_gain, wattn, wconv,
    out, logs,
    tbuf, wbuf, obuf, acc, ssq, kbuf, vbuf, qbuf, qbd, m_ref, a_ref, s_ref, stg, coef,
    csend, crecv, cown, ogate, cpad, tail_out, tail_in, convg, attng, oacc,
    w_sem, t_send, t_recv, ku_send, kd_send, vu_send, vd_send, k_recv, v_recv,
    q_send, q_recv, st_send, st_recv, c_send, c_recv, h_send, h_recv,
    g_send, g_recv, a_send, a_recv,
):
    sp, tp = lax.axis_index("sp"), lax.axis_index("tp")
    z, y = sp // NY, lax.rem(sp, NY)
    x, c = tp // CORES, lax.rem(tp, CORES)

    def at_y(step):
        return (z * NY + lax.rem(y + step, NY), tp)

    def at_z(step):
        return (lax.rem(z + step + NZ, NZ) * NY + y, tp)

    after = (lax.rem(sp + 1, NY * NZ), tp)
    before = (lax.rem(sp + NY * NZ - 1, NY * NZ), tp)

    tokens = TpGather(tok, tbuf, t_send, t_recv, sp, x, c)
    conv = TpGather(convg.at[tp], convg, g_send, g_recv, sp, x, c)
    attn = TpGather(attng.at[tp], attng, a_send, a_recv, sp, x, c)

    loads = [
        pltpu.make_async_copy(w, wbuf.at[:, :, i * VDIM : (i + 1) * VDIM], w_sem.at[i])
        for i, w in enumerate((wq, wk, wv, wo, wi, ws))
    ]
    loads += [
        pltpu.make_async_copy(w, obuf.at[i], w_sem.at[6 + i]) for i, w in enumerate((wattn, wconv))
    ]
    for load in loads:
        load.start()

    barrier = pltpu.get_barrier_semaphore()
    for device in (
        tokens.partner, tokens.left, tokens.right, at_y(1), at_y(2), at_y(3), at_z(1), at_z(-1), before,
    ):
        pl.semaphore_signal(barrier, inc=1, device_id=device, device_id_type=MESH)
    pl.semaphore_wait(barrier, 9)

    tokens.start()

    m_ref[...] = jnp.full_like(m_ref, MASKED)
    a_ref[...] = jnp.zeros_like(a_ref)
    qbd[...] = jnp.zeros_like(qbd)
    acc[...] = jnp.zeros_like(acc)
    ssq[...] = jnp.zeros_like(ssq)
    for load in loads[:6]:
        load.wait()

    def project(slot, h, src=None):
        rows = slice(h * HALF, (h + 1) * HALF)
        block = f32(tbuf[slot, rows] if src is None else src[rows])
        square = block * block
        ssq[rows] += square[:, :128] + square[:, 128:]
        scaled = bf16(block * gain[slot])
        acc[rows] += jnp.dot(scaled, wbuf[slot], preferred_element_type=jnp.float32)

    project(tp, 0, tok)
    project(tp, 1, tok)
    for h in (0, 1):
        tokens.wait(0, True, h)
        project(tokens.slot(0, True), h)
    tokens.neighbours_first()
    project(tokens.slot(-1, False), 0)
    project(tokens.slot(1, False), 1)
    tokens.neighbours_second()
    project(tokens.slot(-1, False), 1)
    project(tokens.slot(1, False), 0)
    for dx, h in ((-1, 0), (1, 1), (-1, 1), (1, 0)):
        tokens.wait(dx, True, h)
        project(tokens.slot(dx, True), h)
    for h in (0, 1):
        tokens.opposite(h)
        project(tokens.slot(2, False), h)
    for h in (0, 1):
        tokens.wait(2, True, h)
        project(tokens.slot(2, True), h)

    total = jnp.sum(ssq[...], axis=1, keepdims=True)
    inverse_rms = lax.rsqrt(total / (NTP * PIECE) + NORM_EPS)

    def projected(i):
        return inverse_rms * acc[:, i * VDIM : (i + 1) * VDIM]

    first_half = lax.rem(lax.broadcasted_iota(jnp.int32, (ROWS, VDIM), 1), DIM) < DIM // 2

    def turned(field):
        other = jnp.where(
            first_half, pltpu.roll(field, VDIM - DIM // 2, 1), pltpu.roll(field, DIM // 2, 1)
        )
        return field * cosine[...] + other * sine[...]

    kbuf[z] = bf16(turned(projected(1)))
    vbuf[z] = bf16(jnp.transpose(projected(2)))

    def k_copy(slot, send_sem, device):
        return remote(kbuf.at[slot], kbuf.at[slot], send_sem, k_recv.at[slot], device)

    def v_copy(slot, send_sem, device):
        return remote(vbuf.at[slot], vbuf.at[slot], send_sem, v_recv.at[slot], device)

    k_copy(z, ku_send.at[0], at_z(1)).start()
    k_copy(z, kd_send.at[0], at_z(-1)).start()
    v_copy(z, vu_send.at[0], at_z(1)).start()
    v_copy(z, vd_send.at[0], at_z(-1)).start()

    qbuf[y] = bf16(jnp.transpose(turned(projected(0))))
    q_copies = [
        remote(qbuf.at[y], qbuf.at[y], q_send.at[i - 1], q_recv.at[y], at_y(i)) for i in (1, 3, 2)
    ]
    for copy in q_copies:
        copy.start()

    ogate[...] = f32(bf16(projected(3)))
    conv_in = bf16(f32(bf16(projected(4))) * f32(bf16(projected(5))))
    cpad[8:] = f32(conv_in)
    tail_out[...] = conv_in[ROWS - 16 :]
    tail = remote(tail_out, tail_in, h_send, h_recv, after)
    tail.start()

    def blocked(block):
        scaled = f32(qbuf[block]) * (LOG2E * DIM**-0.5)
        high = bf16(scaled)
        low = bf16(scaled - f32(high))
        for h in (0, 1):
            lanes = slice(h * TILE, (h + 1) * TILE)
            for t, term in enumerate((high, low)):
                qbd[block * 2 + h, t * VDIM : t * VDIM + DIM, :TILE] = term[:DIM, lanes]
                qbd[block * 2 + h, t * VDIM + DIM : (t + 1) * VDIM, TILE:] = term[DIM:, lanes]

    ones = jnp.ones((ONES_ROWS, ROWS), jnp.bfloat16)

    def scores(slot, tile):
        keys = kbuf[slot]
        return jnp.dot(
            jnp.concatenate([keys, keys], axis=1), qbd[tile], preferred_element_type=jnp.float32
        )

    def absorb(slot, tile, s):
        m_old = m_ref[tile]
        m_new = jnp.maximum(m_old, jnp.max(s, axis=0, keepdims=True))
        keep = jnp.exp2(m_old - m_new)
        m_ref[tile] = m_new
        weights = bf16(jnp.exp2(s - m_new))
        a_ref[tile] = a_ref[tile] * keep + jnp.dot(
            jnp.concatenate([vbuf[slot], ones], axis=0), weights, preferred_element_type=jnp.float32
        )

    def whole_block(slot):
        s_ref[0] = scores(slot, 0)

        @pl.loop(0, TILES // 4)
        def _(g):
            for i in range(4):
                tile = g * 4 + i
                s_ref[(i + 1) % 2] = scores(slot, lax.rem(tile + 1, TILES))
                absorb(slot, tile, s_ref[i % 2])

    blocked(y)
    key_pos = lax.broadcasted_iota(jnp.int32, (ROWS, LANES), 0)
    query_pos = lax.rem(lax.broadcasted_iota(jnp.int32, (ROWS, LANES), 1), TILE)

    @pl.loop(0, 2)
    def _(h):
        s = jnp.where(key_pos <= query_pos + h * TILE, scores(z, y * 2 + h), MASKED)
        absorb(z, y * 2 + h, s)

    for i in (1, 3, 2):
        block = lax.rem(y + i, NY)
        remote(qbuf.at[block], qbuf.at[block], q_send.at[0], q_recv.at[block], at_y(1)).wait_recv()
        blocked(block)

    @pl.loop((y + 1) * 2, TILES)
    def _(tile):
        absorb(z, tile, scores(z, tile))

    tail.wait_recv()
    rim = f32(tail_in[8:])
    cpad[:8] = jnp.where(sp > 0, rim, jnp.zeros_like(rim))
    summed = taps[0:1] * cpad[6 : 6 + ROWS]
    summed += taps[1:2] * cpad[7 : 7 + ROWS]
    summed += taps[2:3] * cpad[8 : 8 + ROWS]
    convg[tp] = bf16(ogate[...] * summed)
    conv.start()

    @pl.loop(1, NZ // 2 + 1)
    def _(d):
        below, above = lax.rem(z - d + NZ, NZ), lax.rem(z + d, NZ)
        last = NZ // 2
        k_copy(below, ku_send.at[0], at_z(1)).wait_recv()

        @pl.when(d < last)
        def _():
            k_copy(below, ku_send.at[d], at_z(1)).start()
            k_copy(above, ku_send.at[0], at_z(1)).wait_recv()

        @pl.when(d < last - 1)
        def _():
            k_copy(above, kd_send.at[d], at_z(-1)).start()

        v_copy(above, vu_send.at[0], at_z(1)).wait_recv()

        @pl.when(d < last)
        def _():
            v_copy(above, vd_send.at[d], at_z(-1)).start()
            v_copy(below, vu_send.at[0], at_z(1)).wait_recv()

        @pl.when(d < last - 1)
        def _():
            v_copy(below, vu_send.at[d], at_z(1)).start()

        @pl.loop(0, 2)
        def _(r):
            source = jnp.where(r == 0, below, above)

            @pl.when((source < z) & ((d < last) | (r == 0)))
            def _():
                whole_block(source)

        @pl.when(d == 1)
        def _():
            conv.neighbours_first()
            conv.neighbours_second()

        @pl.when(d == 2)
        def _():
            conv.opposite(0)
            conv.opposite(1)

    for tile in range(TILES):
        stg[y, 0, tile : tile + 1] = m_ref[tile]
        stg[y, 1, tile : tile + 1] = a_ref[tile, VDIM : VDIM + 1]
    st_copies = [
        remote(stg.at[y], stg.at[y], st_send.at[i - 1], st_recv.at[y], at_y(i)) for i in (1, 3, 2)
    ]
    for copy in st_copies:
        copy.start()

    for load in loads[6:]:
        load.wait()
    for dx, h in ((-1, 0), (1, 1), (-1, 1), (1, 0), (0, 0), (0, 1), (2, 0), (2, 1)):
        conv.wait(dx, True, h)

    def mixed(buf, which, slot, rows):
        return jnp.dot(buf[slot, rows], obuf[which, slot], preferred_element_type=jnp.float32)

    oacc[...] = jnp.zeros_like(oacc)

    @pl.loop(0, NTP)
    def _(slot):
        oacc[...] += mixed(convg, 1, slot, slice(0, ROWS))

    for i in (1, 3, 2):
        peer = lax.rem(y + i, NY)
        remote(stg.at[peer], stg.at[peer], st_send.at[0], st_recv.at[peer], at_y(1)).wait_recv()
    m_all = stg[0, 0]
    for i in range(1, NY):
        m_all = jnp.maximum(m_all, stg[i, 0])
    l_all = stg[0, 1] * jnp.exp2(stg[0, 0] - m_all)
    for i in range(1, NY):
        l_all = l_all + stg[i, 1] * jnp.exp2(stg[i, 0] - m_all)
    second = lax.broadcasted_iota(jnp.int32, (TILES, LANES), 1) >= TILE
    share = jnp.exp2(stg[y, 0] - m_all) / l_all
    coef[0] = jnp.where(second, -lam[...] * share, share)
    coef[1] = m_all * LN2 + jnp.log(l_all)

    def combined(tile):
        part = a_ref[tile, :VDIM] * coef[0, pl.ds(tile, 1)]
        return part[:, :TILE] + part[:, TILE:]

    c_copies = []
    for i in (1, 3, 2):
        block = lax.rem(y + i, NY)
        for h in (0, 1):
            csend[block, :, h * TILE : (h + 1) * TILE] = bf16(combined(block * 2 + h))
        copy = remote(csend.at[block], crecv.at[y], c_send.at[i - 1], c_recv.at[y], at_y(i))
        copy.start()
        c_copies.append(copy)
    for h in (0, 1):
        lanes = slice(h * TILE, (h + 1) * TILE)
        cown[:, lanes] = combined(y * 2 + h)
        row = coef[1, pl.ds(y * 2 + h, 1)]
        logs[0:1, lanes] = row[:, :TILE]
        logs[1:2, lanes] = row[:, TILE:]
    for i in (1, 3, 2):
        peer = lax.rem(y + i, NY)
        remote(csend.at[peer], crecv.at[peer], c_send.at[0], c_recv.at[peer], at_y(1)).wait_recv()
        cown[...] += f32(crecv[peer])

    head_mix = cown[...]
    mean = jnp.sum(head_mix * head_mix, axis=0, keepdims=True) / VDIM
    normed = jnp.transpose(head_mix * lax.rsqrt(mean + HEAD_EPS))
    attng[tp] = bf16(normed * head_gain[...] * HEAD_SCALE)
    attn.start()

    def add(slot, h):
        rows = slice(h * HALF, (h + 1) * HALF)
        oacc[rows] += mixed(attng, 0, slot, rows)

    add(tp, 0)
    add(tp, 1)
    for h in (0, 1):
        attn.wait(0, True, h)
        add(attn.slot(0, True), h)
    attn.neighbours_first()
    add(attn.slot(-1, False), 0)
    add(attn.slot(1, False), 1)
    attn.neighbours_second()
    add(attn.slot(-1, False), 1)
    add(attn.slot(1, False), 0)
    for dx, h in ((-1, 0), (1, 1), (-1, 1), (1, 0)):
        attn.wait(dx, True, h)
        add(attn.slot(dx, True), h)
    for h in (0, 1):
        attn.opposite(h)
        add(attn.slot(2, False), h)
    for h in (0, 1):
        attn.wait(2, True, h)
        add(attn.slot(2, True), h)
    out[...] = bf16(oacc[...])

    tokens.finish()
    for d in range(NZ // 2):
        k_copy(z, ku_send.at[d], at_z(1)).wait_send()
        v_copy(z, vd_send.at[d], at_z(-1)).wait_send()
        if d < NZ // 2 - 1:
            k_copy(z, kd_send.at[d], at_z(-1)).wait_send()
            v_copy(z, vu_send.at[d], at_z(1)).wait_send()
    for copy in q_copies + st_copies + c_copies + [tail]:
        copy.wait_send()
    conv.finish()
    attn.finish()


def per_device(
    tokens,
    norm_gain,
    query_weight,
    key_weight,
    value_weight,
    outer_gate_weight,
    inner_gate_weight,
    conv_input_weight,
    conv_taps,
    lambdas,
    head_gain,
    attn_out_weight,
    conv_out_weight,
):
    half = DIM // 2
    frequency = ROPE_BASE ** (-jnp.arange(half, dtype=jnp.float32) * 2.0 / DIM)
    position = lax.axis_index("sp") * ROWS + jnp.arange(ROWS, dtype=jnp.int32)
    angles = position.astype(jnp.float32)[:, None] * frequency[None, :]
    cosine, sine = jnp.cos(angles), jnp.sin(angles)
    cosine = jnp.concatenate([cosine] * 4, axis=1)
    sine = jnp.concatenate([-sine, sine] * 2, axis=1)

    def in_pieces(weight):
        return weight.reshape(NTP, PIECE, VDIM)

    vmem = pl.BlockSpec(memory_space=pltpu.VMEM)
    anywhere = pl.BlockSpec(memory_space=pl.ANY)
    dma = pltpu.SemaphoreType.DMA
    bf, fl = jnp.bfloat16, jnp.float32
    mixed_out, logs = pl.pallas_call(
        kernel,
        out_shape=(
            jax.ShapeDtypeStruct((ROWS, PIECE), bf),
            jax.ShapeDtypeStruct((2, ROWS), fl),
        ),
        in_specs=[vmem, vmem] + [anywhere] * 6 + [vmem] * 5 + [anywhere] * 2,
        out_specs=(vmem, vmem),
        scratch_shapes=[
            pltpu.VMEM((NTP, ROWS, PIECE), bf),
            pltpu.VMEM((NTP, PIECE, 6 * VDIM), bf),
            pltpu.VMEM((2, NTP, VDIM, PIECE), bf),
            pltpu.VMEM((ROWS, 6 * VDIM), fl),
            pltpu.VMEM((ROWS, 128), fl),
            pltpu.VMEM((NZ, ROWS, VDIM), bf),
            pltpu.VMEM((NZ, VDIM, ROWS), bf),
            pltpu.VMEM((NY, VDIM, ROWS), bf),
            pltpu.VMEM((TILES, 2 * VDIM, LANES), bf),
            pltpu.VMEM((TILES, 1, LANES), fl),
            pltpu.VMEM((TILES, VDIM + ONES_ROWS, LANES), fl),
            pltpu.VMEM((2, ROWS, LANES), fl),
            pltpu.VMEM((NY, 2, TILES, LANES), fl),
            pltpu.VMEM((2, TILES, LANES), fl),
            pltpu.VMEM((NY, VDIM, ROWS), bf),
            pltpu.VMEM((NY, VDIM, ROWS), bf),
            pltpu.VMEM((VDIM, ROWS), fl),
            pltpu.VMEM((ROWS, VDIM), fl),
            pltpu.VMEM((8 + ROWS, VDIM), fl),
            pltpu.VMEM((16, VDIM), bf),
            pltpu.VMEM((16, VDIM), bf),
            pltpu.VMEM((NTP, ROWS, VDIM), bf),
            pltpu.VMEM((NTP, ROWS, VDIM), bf),
            pltpu.VMEM((ROWS, PIECE), fl),
            dma((8,)),
            dma((14,)),
            dma((NTP, 2)),
            dma((NZ // 2,)),
            dma((NZ // 2,)),
            dma((NZ // 2,)),
            dma((NZ // 2,)),
            dma((NZ,)),
            dma((NZ,)),
            dma((NY,)),
            dma((NY,)),
            dma((NY,)),
            dma((NY,)),
            dma((NY,)),
            dma((NY,)),
            dma,
            dma,
            dma((14,)),
            dma((NTP, 2)),
            dma((14,)),
            dma((NTP, 2)),
        ],
        compiler_params=pltpu.CompilerParams(
            collective_id=0, has_side_effects=True, vmem_limit_bytes=60 * 2**20
        ),
    )(
        tokens,
        norm_gain.reshape(NTP, 1, PIECE),
        *(
            in_pieces(w)
            for w in (
                query_weight,
                key_weight,
                value_weight,
                outer_gate_weight,
                inner_gate_weight,
                conv_input_weight,
            )
        ),
        cosine,
        sine,
        conv_taps,
        lambdas.reshape(1, 1),
        head_gain.reshape(1, VDIM),
        attn_out_weight.reshape(NTP, VDIM, PIECE),
        conv_out_weight.reshape(NTP, VDIM, PIECE),
    )
    return mixed_out, logs[None]


def solution(mesh):
    in_specs = (
        P("sp", "tp"),
        P(),
        P(None, "tp"),
        P(None, "tp"),
        P(None, "tp"),
        P(None, "tp"),
        P(None, "tp"),
        P(None, "tp"),
        P(None, "tp"),
        P("tp"),
        P(),
        P(None, "tp"),
        P(None, "tp"),
    )
    out_specs = (P("sp", "tp"), P("tp", None, "sp"))
    return jax.shard_map(
        per_device, mesh=mesh, in_specs=in_specs, out_specs=out_specs, check_vma=False
    )
```

time: 338 us -> 81.5 us (0.24); the launches traced: 333 us -> 80.1 us
  waiting for transfers between devices: 145 us -> 0 us
  matrix products: 88.6 us -> 0 us
  Pallas kernels: 0 us -> 74.3 us
  other arithmetic: 34.2 us -> 2.26 us
  local copies, waits for them, and re-layouts: 31.1 us -> 2.27 us
  between operations: 14.3 us -> 1.32 us
  loops' own time: 11.4 us -> 0 us
  starting transfers between devices: 8.21 us -> 0 us
    all_gather x2 -> x0, waiting for transfers between devices: 116 us -> none  [the longest x1 84.1 us: side_by_side(): out, at, outs = (lax.all_gather(both, axis, axis=dim, tiled=True), 0, [])]
    dot_general x32 -> x0, matrix products: 88.6 us -> none  [the longest x16 57.3 us: block_scores(): jnp.einsum('qhcd,khcd->hcqk', queries, key_block, preferred_element_type=...]
    pallas_call x0 -> x1, Pallas kernels: none -> 74.3 us  [per_device(): pl.pallas_call(kernel, out_shape=(jax.ShapeDtypeStruct((ROWS, PIECE), bf)...]
    all_to_all x1 -> x0, waiting for transfers between devices: 25.9 us -> none  [from_everyone(): lax.all_to_all(jnp.broadcast_to(x[None], (peers, *x.shape)), axis, 0, 0,...]
    reduce_sum x10 -> x0, other arithmetic: 18.6 us -> none  [the longest x8 18 us: stats_step(): jnp.sum(exponent, axis=-1)]
    unnamed x22 -> x4, local copies, waits for them, and re-layouts: 15.1 us -> 2.27 us
    ge x16 -> x0, other arithmetic: 12.2 us -> none  [block_scores(): query_pos[:, None]]
    another operation x2 -> x0, loops' own time: 11.4 us -> none  [over_shards(): lax.scan(scan_step, running, (stacked, jnp.arange(steps_count, dtype=jnp....]
  transfers between devices with their start and end apart: 4 -> 0, of which waited for: 4 -> 0; matrix products, arithmetic and copies ran while one was open for 2% -> 0% of each run, Pallas kernels for 0% -> 0%
where the time goes in v1:
time: 81.5 us; the launch traced here: 80.1 us
  Pallas kernels  74.3 us (91%)
  local copies, waits for them, and re-layouts  2.27 us (3%)
  other arithmetic  2.26 us (3%)
  between operations  1.32 us (2%)
    pallas_call x1, Pallas kernels, per_device(): pl.pallas_call(kernel, out_shape=(jax.ShapeDtypeStruct((ROWS, PIECE), bf)...  74.3 us
    unnamed x4, local copies, waits for them, and re-layouts  2.27 us

profile of v1, /device:TPU:225, one launch (start us, length us, event | category | flops | bytes accessed | tf_op | source)
XLA Modules:
  0.0 80.1 jit_solution(10431106905184944843)
XLA Ops:
  0.7 1.0 %fusion = (f32[512,32]{1,0:T(8,128)S(1)}, f32[512,32]{1,0:T(8,128)S(1)}, f32[512,32]{1,0:T(8,128)S(1)}) fusion(f32[32]{0:T(128)S(1)} %multiply_power_fusion, f32[512]{0:T(512)S(1)} %add_convert_fusion), kind=kLoop, calls=%fused_computation.4 | loop fusion | flops 32768 | bytes 198784 | tf_op jit(solution)/shard_map/neg | solution.py:467
  1.7 1.3 %pad_maximum_fusion = (f32[512,128]{1,0:T(8,128)}, f32[512,128]{1,0:T(8,128)}) fusion(f32[512,32]{1,0:T(8,128)S(1)} %get-tuple-element.8, f32[512,32]{1,0:T(8,128)S(1)} %get-tuple-element.7, f32[512,32]{1,0:T(8,128)S(1)} %get-tuple-element.6), kind=kLoop, calls=%fused_computation.2 | loop fusion | flops 393216 | bytes 720896 | tf_op jit(solution)/shard_map/concatenate | solution.py:466
  3.6 74.3 %shard_map.140 = (bf16[512,256]{1,0:T(8,128)(2,1)}, f32[2,512]{1,0:T(2,128)}) custom-call(bf16[512,256]{1,0:T(8,128)(2,1)} %tok.1, f32[8,1,256]{2,1,0:T(1,128)} %bitcast.21, bf16[8,256,128]{2,1,0:T(8,128)(2,1)} %bitcast.13, bf16[8,256,128]{2,1,0:T(8,128)(2,1)} %bitcast.14, bf16[8,256,128]{2,1,0:T(8,128)(2,1)} %bitcast.15, bf16[8,256,128]{2,1,0:T(8,128)(2,1)} %bitcast.16, ...), custom_call_target="tpu_custom_call" | custom-call | tf_op jit(solution)/shard_map/pallas_call | solution.py:476
  77.8 0.0 copy-start
  77.9 1.7 %copy.19 = bf16[512,256]{1,0:T(8,128)(2,1)} copy(bf16[512,256]{1,0:T(8,128)(2,1)} %get-tuple-element.13) | data formatting | bytes 524288
  79.5 0.0 copy-done
  79.5 0.6 copy.20
  (2 shorter events, 0.0 us)
Async XLA Ops:
  77.8 1.7 %copy-start = (f32[2,512]{1,0:T(2,128)S(1)}, f32[2,512]{1,0:T(2,128)}, u32[]{:S(2)}) copy-start(f32[2,512]{1,0:T(2,128)} %get-tuple-element.5) | copy-start | bytes 12292

commit v2 on v1

--- a/solution.py
+++ b/solution.py
@@ -2,6 +2,7 @@
 
 import jax
 import jax.numpy as jnp
+import numpy as np
 from jax import lax
 from jax.experimental import pallas as pl
 from jax.experimental.pallas import tpu as pltpu
@@ -106,11 +107,12 @@
 
 
 def kernel(
-    tok, gain, wq, wk, wv, wo, wi, ws, cosine, sine, taps, lam, head_gain, wattn, wconv,
+    tok_in, gain_in, wq, wk, wv, wo, wi, ws, base_in, rows_in, taps_in, lam_in, head_gain_in,
+    wattn, wconv,
     out, logs,
-    tbuf, wbuf, obuf, acc, ssq, kbuf, vbuf, qbuf, qbd, m_ref, a_ref, s_ref, stg, coef,
-    csend, crecv, cown, ogate, cpad, tail_out, tail_in, convg, attng, oacc,
-    w_sem, t_send, t_recv, ku_send, kd_send, vu_send, vd_send, k_recv, v_recv,
+    tok, gain, base, turn, taps, lam, head_gain, tbuf, wbuf, obuf, acc, ssq, kbuf, vbuf, qbuf, qbd, m_ref, a_ref, s_ref, stg, coef,
+    csend, crelay, crecv, cown, ogate, cpad, tail_out, tail_in, convg, attng, oacc,
+    w_sem, i_sem, t_send, t_recv, ku_send, kd_send, vu_send, vd_send, k_recv, v_recv,
     q_send, q_recv, st_send, st_recv, c_send, c_recv, h_send, h_recv,
     g_send, g_recv, a_send, a_recv,
 ):
@@ -131,6 +133,26 @@
     conv = TpGather(convg.at[tp], convg, g_send, g_recv, sp, x, c)
     attn = TpGather(attng.at[tp], attng, a_send, a_recv, sp, x, c)
 
+    barrier = pltpu.get_barrier_semaphore()
+    for device in (
+        tokens.partner, tokens.left, tokens.right, at_y(1), at_y(2), at_y(3), at_z(1), at_z(-1), before,
+    ):
+        pl.semaphore_signal(barrier, inc=1, device_id=device, device_id_type=MESH)
+
+    inputs = [
+        pltpu.make_async_copy(source, target, i_sem.at[i])
+        for i, (source, target) in enumerate(
+            (
+                (tok_in, tok),
+                (gain_in, gain),
+                (base_in.at[sp], base),
+                (rows_in, turn),
+                (taps_in, taps),
+                (lam_in, lam),
+                (head_gain_in, head_gain),
+            )
+        )
+    ]
     loads = [
         pltpu.make_async_copy(w, wbuf.at[:, :, i * VDIM : (i + 1) * VDIM], w_sem.at[i])
         for i, w in enumerate((wq, wk, wv, wo, wi, ws))
@@ -138,14 +160,9 @@
     loads += [
         pltpu.make_async_copy(w, obuf.at[i], w_sem.at[6 + i]) for i, w in enumerate((wattn, wconv))
     ]
-    for load in loads:
+    for load in inputs + loads:
         load.start()
-
-    barrier = pltpu.get_barrier_semaphore()
-    for device in (
-        tokens.partner, tokens.left, tokens.right, at_y(1), at_y(2), at_y(3), at_z(1), at_z(-1), before,
-    ):
-        pl.semaphore_signal(barrier, inc=1, device_id=device, device_id_type=MESH)
+    inputs[0].wait()
     pl.semaphore_wait(barrier, 9)
 
     tokens.start()
@@ -155,8 +172,13 @@
     qbd[...] = jnp.zeros_like(qbd)
     acc[...] = jnp.zeros_like(acc)
     ssq[...] = jnp.zeros_like(ssq)
-    for load in loads[:6]:
+    for load in inputs[1:] + loads[:6]:
         load.wait()
+
+    block_cos, block_sin, signed_cos, signed_sin = (base[i : i + 1] for i in range(4))
+    row_cos, row_sin = turn[0], turn[1]
+    turn[0] = block_cos * row_cos - block_sin * row_sin
+    turn[1] = signed_sin * row_cos + signed_cos * row_sin
 
     def project(slot, h, src=None):
         rows = slice(h * HALF, (h + 1) * HALF)
@@ -199,7 +221,7 @@
         other = jnp.where(
             first_half, pltpu.roll(field, VDIM - DIM // 2, 1), pltpu.roll(field, DIM // 2, 1)
         )
-        return field * cosine[...] + other * sine[...]
+        return field * turn[0] + other * turn[1]
 
     kbuf[z] = bf16(turned(projected(1)))
     vbuf[z] = bf16(jnp.transpose(projected(2)))
@@ -276,14 +298,40 @@
         s = jnp.where(key_pos <= query_pos + h * TILE, scores(z, y * 2 + h), MASKED)
         absorb(z, y * 2 + h, s)
 
+    last = NZ // 2
+
+    def pass_keys(d):
+        below, above = lax.rem(z - d + NZ, NZ), lax.rem(z + d, NZ)
+        k_copy(below, ku_send.at[0], at_z(1)).wait_recv()
+
+        @pl.when(d < last)
+        def _():
+            k_copy(below, ku_send.at[d], at_z(1)).start()
+            k_copy(above, ku_send.at[0], at_z(1)).wait_recv()
+
+        @pl.when(d < last - 1)
+        def _():
+            k_copy(above, kd_send.at[d], at_z(-1)).start()
+
+    def pass_values(d):
+        below, above = lax.rem(z - d + NZ, NZ), lax.rem(z + d, NZ)
+        v_copy(above, vu_send.at[0], at_z(1)).wait_recv()
+
+        @pl.when(d < last)
+        def _():
+            v_copy(above, vd_send.at[d], at_z(-1)).start()
+            v_copy(below, vu_send.at[0], at_z(1)).wait_recv()
+
+        @pl.when(d < last - 1)
+        def _():
+            v_copy(below, vu_send.at[d], at_z(1)).start()
+
     for i in (1, 3, 2):
         block = lax.rem(y + i, NY)
         remote(qbuf.at[block], qbuf.at[block], q_send.at[0], q_recv.at[block], at_y(1)).wait_recv()
         blocked(block)
-
-    @pl.loop((y + 1) * 2, TILES)
-    def _(tile):
-        absorb(z, tile, scores(z, tile))
+        if i == 3:
+            pass_keys(1)
 
     tail.wait_recv()
     rim = f32(tail_in[8:])
@@ -294,46 +342,38 @@
     convg[tp] = bf16(ogate[...] * summed)
     conv.start()
 
-    @pl.loop(1, NZ // 2 + 1)
-    def _(d):
-        below, above = lax.rem(z - d + NZ, NZ), lax.rem(z + d, NZ)
-        last = NZ // 2
-        k_copy(below, ku_send.at[0], at_z(1)).wait_recv()
-
-        @pl.when(d < last)
-        def _():
-            k_copy(below, ku_send.at[d], at_z(1)).start()
-            k_copy(above, ku_send.at[0], at_z(1)).wait_recv()
-
-        @pl.when(d < last - 1)
-        def _():
-            k_copy(above, kd_send.at[d], at_z(-1)).start()
-
-        v_copy(above, vu_send.at[0], at_z(1)).wait_recv()
-
-        @pl.when(d < last)
-        def _():
-            v_copy(above, vd_send.at[d], at_z(-1)).start()
-            v_copy(below, vu_send.at[0], at_z(1)).wait_recv()
-
-        @pl.when(d < last - 1)
-        def _():
-            v_copy(below, vu_send.at[d], at_z(1)).start()
-
-        @pl.loop(0, 2)
-        def _(r):
-            source = jnp.where(r == 0, below, above)
-
-            @pl.when((source < z) & ((d < last) | (r == 0)))
-            def _():
-                whole_block(source)
-
-        @pl.when(d == 1)
+    @pl.loop(y + 1, NY)
+    def _(block):
+        for h in (0, 1):
+            s_ref[h] = scores(z, block * 2 + h)
+        for h in (0, 1):
+            absorb(z, block * 2 + h, s_ref[h])
+
+    pass_values(1)
+
+    @pl.loop(0, NZ - 1)
+    def _(i):
+        d, r = i // 2 + 1, lax.rem(i, 2)
+        source = lax.rem(z + jnp.where(r == 0, NZ - d, d), NZ)
+
+        @pl.when(source < z)
+        def _():
+            whole_block(source)
+
+        @pl.when((r == 0) & (d < last))
+        def _():
+            pass_keys(d + 1)
+
+        @pl.when(r == 1)
+        def _():
+            pass_values(d + 1)
+
+        @pl.when(i == 1)
         def _():
             conv.neighbours_first()
             conv.neighbours_second()
 
-        @pl.when(d == 2)
+        @pl.when(i == 3)
         def _():
             conv.opposite(0)
             conv.opposite(1)
@@ -372,31 +412,49 @@
         l_all = l_all + stg[i, 1] * jnp.exp2(stg[i, 0] - m_all)
     second = lax.broadcasted_iota(jnp.int32, (TILES, LANES), 1) >= TILE
     share = jnp.exp2(stg[y, 0] - m_all) / l_all
-    coef[0] = jnp.where(second, -lam[...] * share, share)
+    coef[0] = jnp.where(second, -lam[0:1, 0:1] * share, share)
     coef[1] = m_all * LN2 + jnp.log(l_all)
 
     def combined(tile):
         part = a_ref[tile, :VDIM] * coef[0, pl.ds(tile, 1)]
         return part[:, :TILE] + part[:, TILE:]
 
+    right, left = lax.rem(y + 1, NY), lax.rem(y + 3, NY)
+    opposite = lax.rem(y + 2, NY)
+    to = (at_y(1), at_y(-1 + NY))
+    near = (right, left)
     c_copies = []
-    for i in (1, 3, 2):
-        block = lax.rem(y + i, NY)
-        for h in (0, 1):
-            csend[block, :, h * TILE : (h + 1) * TILE] = bf16(combined(block * 2 + h))
-        copy = remote(csend.at[block], crecv.at[y], c_send.at[i - 1], c_recv.at[y], at_y(i))
+
+    def send_part(i, target, device):
+        copy = remote(csend.at[i], target, c_send.at[i], c_recv.at[i], device)
         copy.start()
         c_copies.append(copy)
+
+    for w in (0, 1):
+        csend[w] = bf16(combined(opposite * 2 + w))
+    for w in (0, 1):
+        send_part(w, crelay.at[w], to[w])
+    for w in (0, 1):
+        csend[2 + w] = bf16(combined(near[w] * 2 + 1 - w))
+    for w in (0, 1):
+        send_part(2 + w, crecv.at[w, 0], to[w])
+    relayed = [combined(near[w] * 2 + w) for w in (0, 1)]
+    for w in (0, 1):
+        c_copies[w].wait_recv()
+        csend[4 + w] = bf16(relayed[w] + f32(crelay[w]))
+        send_part(4 + w, crecv.at[w, 1], to[w])
     for h in (0, 1):
         lanes = slice(h * TILE, (h + 1) * TILE)
         cown[:, lanes] = combined(y * 2 + h)
         row = coef[1, pl.ds(y * 2 + h, 1)]
-        logs[0:1, lanes] = row[:, :TILE]
-        logs[1:2, lanes] = row[:, TILE:]
-    for i in (1, 3, 2):
-        peer = lax.rem(y + i, NY)
-        remote(csend.at[peer], crecv.at[peer], c_send.at[0], c_recv.at[peer], at_y(1)).wait_recv()
-        cown[...] += f32(crecv[peer])
+        logs[0, 0:1, lanes] = row[:, :TILE]
+        logs[0, 1:2, lanes] = row[:, TILE:]
+    for w in (0, 1):
+        c_copies[2 + w].wait_recv()
+        cown[:, (1 - w) * TILE : (2 - w) * TILE] += f32(crecv[w, 0])
+    for w in (0, 1):
+        c_copies[4 + w].wait_recv()
+        cown[:, w * TILE : (w + 1) * TILE] += f32(crecv[w, 1])
 
     head_mix = cown[...]
     mean = jnp.sum(head_mix * head_mix, axis=0, keepdims=True) / VDIM
@@ -459,29 +517,38 @@
     conv_out_weight,
 ):
     half = DIM // 2
-    frequency = ROPE_BASE ** (-jnp.arange(half, dtype=jnp.float32) * 2.0 / DIM)
-    position = lax.axis_index("sp") * ROWS + jnp.arange(ROWS, dtype=jnp.int32)
-    angles = position.astype(jnp.float32)[:, None] * frequency[None, :]
-    cosine, sine = jnp.cos(angles), jnp.sin(angles)
-    cosine = jnp.concatenate([cosine] * 4, axis=1)
-    sine = jnp.concatenate([-sine, sine] * 2, axis=1)
+    frequency = np.float32(ROPE_BASE) ** (-np.arange(half, dtype=np.float32) * 2.0 / DIM)
+    frequency = np.tile(frequency.astype(np.float64), 4)
+    sign = np.tile(np.repeat([-1.0, 1.0], half), 2)
+    start = np.arange(NY * NZ)[:, None] * ROWS * frequency
+    cosine, sine = np.cos(start), np.sin(start)
+    base = np.stack([cosine, sine, sign * cosine, sign * sine], axis=1).astype(np.float32)
+    row = np.arange(ROWS)[:, None] * frequency
+    rows = np.stack([np.cos(row), np.sin(row)]).astype(np.float32)
 
     def in_pieces(weight):
         return weight.reshape(NTP, PIECE, VDIM)
 
     vmem = pl.BlockSpec(memory_space=pltpu.VMEM)
-    anywhere = pl.BlockSpec(memory_space=pl.ANY)
+    anywhere = pl.BlockSpec(memory_space=pltpu.HBM)
     dma = pltpu.SemaphoreType.DMA
     bf, fl = jnp.bfloat16, jnp.float32
     mixed_out, logs = pl.pallas_call(
         kernel,
         out_shape=(
             jax.ShapeDtypeStruct((ROWS, PIECE), bf),
-            jax.ShapeDtypeStruct((2, ROWS), fl),
+            jax.ShapeDtypeStruct((1, 2, ROWS), fl),
         ),
-        in_specs=[vmem, vmem] + [anywhere] * 6 + [vmem] * 5 + [anywhere] * 2,
+        in_specs=[anywhere] * 15,
         out_specs=(vmem, vmem),
         scratch_shapes=[
+            pltpu.VMEM((ROWS, PIECE), bf),
+            pltpu.VMEM((NTP, 1, PIECE), fl),
+            pltpu.VMEM((4, 128), fl),
+            pltpu.VMEM((2, ROWS, 128), fl),
+            pltpu.VMEM((3, VDIM), fl),
+            pltpu.VMEM((1, 128), fl),
+            pltpu.VMEM((1, VDIM), fl),
             pltpu.VMEM((NTP, ROWS, PIECE), bf),
             pltpu.VMEM((NTP, PIECE, 6 * VDIM), bf),
             pltpu.VMEM((2, NTP, VDIM, PIECE), bf),
@@ -496,8 +563,9 @@
             pltpu.VMEM((2, ROWS, LANES), fl),
             pltpu.VMEM((NY, 2, TILES, LANES), fl),
             pltpu.VMEM((2, TILES, LANES), fl),
-            pltpu.VMEM((NY, VDIM, ROWS), bf),
-            pltpu.VMEM((NY, VDIM, ROWS), bf),
+            pltpu.VMEM((6, VDIM, TILE), bf),
+            pltpu.VMEM((2, VDIM, TILE), bf),
+            pltpu.VMEM((2, 2, VDIM, TILE), bf),
             pltpu.VMEM((VDIM, ROWS), fl),
             pltpu.VMEM((ROWS, VDIM), fl),
             pltpu.VMEM((8 + ROWS, VDIM), fl),
@@ -507,6 +575,7 @@
             pltpu.VMEM((NTP, ROWS, VDIM), bf),
             pltpu.VMEM((ROWS, PIECE), fl),
             dma((8,)),
+            dma((7,)),
             dma((14,)),
             dma((NTP, 2)),
             dma((NZ // 2,)),
@@ -519,8 +588,8 @@
             dma((NY,)),
             dma((NY,)),
             dma((NY,)),
-            dma((NY,)),
-            dma((NY,)),
+            dma((6,)),
+            dma((6,)),
             dma,
             dma,
             dma((14,)),
@@ -545,15 +614,15 @@
                 conv_input_weight,
             )
         ),
-        cosine,
-        sine,
+        jnp.asarray(base),
+        jnp.asarray(rows),
         conv_taps,
-        lambdas.reshape(1, 1),
+        jnp.broadcast_to(lambdas, (1, 128)),
         head_gain.reshape(1, VDIM),
         attn_out_weight.reshape(NTP, VDIM, PIECE),
         conv_out_weight.reshape(NTP, VDIM, PIECE),
     )
-    return mixed_out, logs[None]
+    return mixed_out, logs
 
 
 def solution(mesh):

time: 81.5 us -> 74.5 us (0.914)
  Pallas kernels: 74.3 us -> 69.8 us
  other arithmetic: 2.26 us -> 0 us
    pallas_call x1, Pallas kernels: 74.3 us -> 69.8 us  [per_device(): pl.pallas_call(kernel, out_shape=(jax.ShapeDtypeStruct((ROWS, PIECE), bf)...]
    concatenate x1 -> x0, other arithmetic: 1.25 us -> none  [per_device(): cosine = jnp.concatenate([cosine] * 4, axis=1)]
    neg x1 -> x0, other arithmetic: 0.99 us -> none  [per_device(): sine = jnp.concatenate([-sine, sine] * 2, axis=1)]
where the time goes in v2:
time: 74.5 us; the launch traced here: 73.8 us
  Pallas kernels  69.8 us (94%)
  local copies, waits for them, and re-layouts  2.78 us (4%)
  between operations  1.29 us (2%)
    pallas_call x1, Pallas kernels, per_device(): pl.pallas_call(kernel, out_shape=(jax.ShapeDtypeStruct((ROWS, PIECE), bf)...  69.8 us
    unnamed x4, local copies, waits for them, and re-layouts  2.27 us

profile of v2, /device:TPU:225, one launch (start us, length us, event | category | flops | bytes accessed | tf_op | source)
XLA Modules:
  0.0 73.8 jit_solution(9571788093177856061)
XLA Ops:
  1.3 0.5 broadcast_in_dim.2.lam_in
  1.8 69.8 %shard_map.161 = (bf16[512,256]{1,0:T(8,128)(2,1)}, f32[1,2,512]{2,1,0:T(2,128)}) custom-call(bf16[512,256]{1,0:T(8,128)(2,1)} %tok_in.1, f32[8,1,256]{2,1,0:T(1,128)} %bitcast.20, bf16[8,256,128]{2,1,0:T(8,128)(2,1)} %bitcast.12, bf16[8,256,128]{2,1,0:T(8,128)(2,1)} %bitcast.13, bf16[8,256,128]{2,1,0:T(8,128)(2,1)} %bitcast.14, ...), custom_call_target="tpu_custom_call" | custom-call | tf_op jit(solution)/shard_map/pallas_call | solution.py:536
  71.6 0.0 copy-start
  71.6 1.7 %copy.20 = bf16[512,256]{1,0:T(8,128)(2,1)} copy(bf16[512,256]{1,0:T(8,128)(2,1)} %get-tuple-element.4) | data formatting | bytes 524288
  73.2 0.0 copy-done
  73.2 0.6 copy.21
Async XLA Ops:
  71.6 1.7 %copy-start = (f32[1,2,512]{2,1,0:T(2,128)S(1)}, f32[1,2,512]{2,1,0:T(2,128)}, u32[]{:S(2)}) copy-start(f32[1,2,512]{2,1,0:T(2,128)} %get-tuple-element.5) | copy-start | bytes 12292

commit v3 on v2

--- a/solution.py
+++ b/solution.py
@@ -50,55 +50,63 @@
 
 
 class TpGather:
-    def __init__(self, own, buf, send, recv, sp, x, c):
-        self.own, self.buf, self.send, self.recv = own, buf, send, recv
+    def __init__(self, own, buf, send, recv, parts, sp, x, c):
+        self.own, self.buf, self.send, self.recv, self.parts = own, buf, send, recv, parts
         self.slot = lambda dx, other: lax.rem(x + dx + NX, NX) * CORES + (1 - c if other else c)
         self.partner = (sp, x * CORES + 1 - c)
         self.right = (sp, self.slot(1, False))
         self.left = (sp, self.slot(-1, False))
         self.started = 0
 
-    def rows(self, h):
-        half = self.buf.shape[1] // 2
-        return pl.ds(h * half, half)
-
-    def push(self, dx, h, device, first=False):
+    def rows(self, p):
+        size = self.buf.shape[1] // self.parts
+        return pl.ds(p * size, size)
+
+    def push(self, dx, p, device, first=False):
         slot = self.slot(dx, False)
-        block = self.buf.at[slot, self.rows(h)]
-        source = self.own.at[self.rows(h)] if first else block
-        remote(source, block, self.send.at[self.started], self.recv.at[slot, h], device).start()
+        block = self.buf.at[slot, self.rows(p)]
+        source = self.own.at[self.rows(p)] if first else block
+        remote(source, block, self.send.at[self.started], self.recv.at[slot, p], device).start()
         self.started += 1
 
-    def wait(self, dx, other, h):
+    def wait(self, dx, other, *parts):
         slot = self.slot(dx, other)
-        block = self.buf.at[slot, self.rows(h)]
-        remote(block, block, self.send.at[0], self.recv.at[slot, h], self.partner).wait_recv()
-
-    def start(self):
-        self.push(0, 0, self.right, True)
-        self.push(0, 1, self.left, True)
-        self.push(0, 1, self.right, True)
-        self.push(0, 0, self.left, True)
-        self.push(0, 0, self.partner, True)
-        self.push(0, 1, self.partner, True)
-
-    def neighbours_first(self):
-        self.wait(-1, False, 0)
-        self.push(-1, 0, self.right)
-        self.push(-1, 0, self.partner)
-        self.wait(1, False, 1)
-        self.push(1, 1, self.left)
-        self.push(1, 1, self.partner)
-
-    def neighbours_second(self):
-        self.wait(-1, False, 1)
-        self.push(-1, 1, self.partner)
-        self.wait(1, False, 0)
-        self.push(1, 0, self.partner)
-
-    def opposite(self, h):
-        self.wait(2, False, h)
-        self.push(2, h, self.partner)
+        for p in parts:
+            block = self.buf.at[slot, self.rows(p)]
+            remote(block, block, self.send.at[0], self.recv.at[slot, p], self.partner).wait_recv()
+
+    def start(self, *pairs):
+        for p in pairs:
+            self.push(0, p, self.right, True)
+            self.push(0, p + 1, self.left, True)
+        for p in pairs:
+            self.push(0, p + 1, self.right, True)
+            self.push(0, p, self.left, True)
+        for p in pairs:
+            self.push(0, p, self.partner, True)
+            self.push(0, p + 1, self.partner, True)
+
+    def neighbours_first(self, *pairs):
+        for p in pairs:
+            self.wait(-1, False, p)
+            self.push(-1, p, self.right)
+            self.wait(1, False, p + 1)
+            self.push(1, p + 1, self.left)
+        for p in pairs:
+            self.push(-1, p, self.partner)
+            self.push(1, p + 1, self.partner)
+
+    def neighbours_second(self, *pairs):
+        for p in pairs:
+            self.wait(-1, False, p + 1)
+            self.push(-1, p + 1, self.partner)
+            self.wait(1, False, p)
+            self.push(1, p, self.partner)
+
+    def opposite(self, *parts):
+        for p in parts:
+            self.wait(2, False, p)
+            self.push(2, p, self.partner)
 
     def finish(self):
         block = self.buf.at[0, self.rows(0)]
@@ -129,9 +137,9 @@
     after = (lax.rem(sp + 1, NY * NZ), tp)
     before = (lax.rem(sp + NY * NZ - 1, NY * NZ), tp)
 
-    tokens = TpGather(tok, tbuf, t_send, t_recv, sp, x, c)
-    conv = TpGather(convg.at[tp], convg, g_send, g_recv, sp, x, c)
-    attn = TpGather(attng.at[tp], attng, a_send, a_recv, sp, x, c)
+    tokens = TpGather(tok, tbuf, t_send, t_recv, 2, sp, x, c)
+    conv = TpGather(convg.at[tp], convg, g_send, g_recv, 2, sp, x, c)
+    attn = TpGather(attng.at[tp], attng, a_send, a_recv, 4, sp, x, c)
 
     barrier = pltpu.get_barrier_semaphore()
     for device in (
@@ -165,7 +173,7 @@
     inputs[0].wait()
     pl.semaphore_wait(barrier, 9)
 
-    tokens.start()
+    tokens.start(0)
 
     m_ref[...] = jnp.full_like(m_ref, MASKED)
     a_ref[...] = jnp.zeros_like(a_ref)
@@ -188,26 +196,32 @@
         scaled = bf16(block * gain[slot])
         acc[rows] += jnp.dot(scaled, wbuf[slot], preferred_element_type=jnp.float32)
 
+    def gathered(gather, use):
+        each = gather.parts // 2
+        halves = (range(each), range(each, 2 * each))
+        pairs = range(0, gather.parts, 2)
+        for h in (0, 1):
+            gather.wait(0, True, *halves[h])
+            use(gather.slot(0, True), h)
+        gather.neighbours_first(*pairs)
+        gather.neighbours_second(*pairs)
+        for dx in (-1, 1):
+            for h in (0, 1):
+                use(gather.slot(dx, False), h)
+        for dx in (-1, 1):
+            for h in (0, 1):
+                gather.wait(dx, True, *halves[h])
+                use(gather.slot(dx, True), h)
+        gather.opposite(*halves[0], *halves[1])
+        for other in (False, True):
+            for h in (0, 1):
+                if other:
+                    gather.wait(2, True, *halves[h])
+                use(gather.slot(2, other), h)
+
     project(tp, 0, tok)
     project(tp, 1, tok)
-    for h in (0, 1):
-        tokens.wait(0, True, h)
-        project(tokens.slot(0, True), h)
-    tokens.neighbours_first()
-    project(tokens.slot(-1, False), 0)
-    project(tokens.slot(1, False), 1)
-    tokens.neighbours_second()
-    project(tokens.slot(-1, False), 1)
-    project(tokens.slot(1, False), 0)
-    for dx, h in ((-1, 0), (1, 1), (-1, 1), (1, 0)):
-        tokens.wait(dx, True, h)
-        project(tokens.slot(dx, True), h)
-    for h in (0, 1):
-        tokens.opposite(h)
-        project(tokens.slot(2, False), h)
-    for h in (0, 1):
-        tokens.wait(2, True, h)
-        project(tokens.slot(2, True), h)
+    gathered(tokens, project)
 
     total = jnp.sum(ssq[...], axis=1, keepdims=True)
     inverse_rms = lax.rsqrt(total / (NTP * PIECE) + NORM_EPS)
@@ -258,45 +272,42 @@
         for h in (0, 1):
             lanes = slice(h * TILE, (h + 1) * TILE)
             for t, term in enumerate((high, low)):
-                qbd[block * 2 + h, t * VDIM : t * VDIM + DIM, :TILE] = term[:DIM, lanes]
-                qbd[block * 2 + h, t * VDIM + DIM : (t + 1) * VDIM, TILE:] = term[DIM:, lanes]
+                qbd[h * NY + block, t * VDIM : t * VDIM + DIM, :TILE] = term[:DIM, lanes]
+                qbd[h * NY + block, t * VDIM + DIM : (t + 1) * VDIM, TILE:] = term[DIM:, lanes]
 
     ones = jnp.ones((ONES_ROWS, ROWS), jnp.bfloat16)
 
-    def scores(slot, tile):
-        keys = kbuf[slot]
+    def scores(slot, tile, count=ROWS):
+        keys = kbuf[slot, :count]
         return jnp.dot(
             jnp.concatenate([keys, keys], axis=1), qbd[tile], preferred_element_type=jnp.float32
         )
 
-    def absorb(slot, tile, s):
+    def absorb(slot, tile, s, count=ROWS):
         m_old = m_ref[tile]
         m_new = jnp.maximum(m_old, jnp.max(s, axis=0, keepdims=True))
         keep = jnp.exp2(m_old - m_new)
         m_ref[tile] = m_new
         weights = bf16(jnp.exp2(s - m_new))
         a_ref[tile] = a_ref[tile] * keep + jnp.dot(
-            jnp.concatenate([vbuf[slot], ones], axis=0), weights, preferred_element_type=jnp.float32
+            jnp.concatenate([vbuf[slot, :, :count], ones[:, :count]], axis=0),
+            weights,
+            preferred_element_type=jnp.float32,
         )
 
-    def whole_block(slot):
-        s_ref[0] = scores(slot, 0)
-
-        @pl.loop(0, TILES // 4)
-        def _(g):
-            for i in range(4):
-                tile = g * 4 + i
-                s_ref[(i + 1) % 2] = scores(slot, lax.rem(tile + 1, TILES))
-                absorb(slot, tile, s_ref[i % 2])
+    def four_tiles(slot, g):
+        for i in range(4):
+            tile = g * 4 + i
+            s_ref[(i + 1) % 2] = scores(slot, lax.rem(tile + 1, TILES))
+            absorb(slot, tile, s_ref[i % 2])
 
     blocked(y)
-    key_pos = lax.broadcasted_iota(jnp.int32, (ROWS, LANES), 0)
-    query_pos = lax.rem(lax.broadcasted_iota(jnp.int32, (ROWS, LANES), 1), TILE)
-
-    @pl.loop(0, 2)
-    def _(h):
-        s = jnp.where(key_pos <= query_pos + h * TILE, scores(z, y * 2 + h), MASKED)
-        absorb(z, y * 2 + h, s)
+    for h in (0, 1):
+        count = (h + 1) * TILE
+        key_pos = lax.broadcasted_iota(jnp.int32, (count, LANES), 0)
+        query_pos = lax.rem(lax.broadcasted_iota(jnp.int32, (count, LANES), 1), TILE) + h * TILE
+        s = jnp.where(key_pos <= query_pos, scores(z, h * NY + y, count), MASKED)
+        absorb(z, h * NY + y, s, count)
 
     last = NZ // 2
 
@@ -325,13 +336,26 @@
         @pl.when(d < last - 1)
         def _():
             v_copy(below, vu_send.at[d], at_z(1)).start()
+
+    pass_keys(1)
 
     for i in (1, 3, 2):
         block = lax.rem(y + i, NY)
         remote(qbuf.at[block], qbuf.at[block], q_send.at[0], q_recv.at[block], at_y(1)).wait_recv()
         blocked(block)
-        if i == 3:
-            pass_keys(1)
+
+    @pl.when(y < NY - 1)
+    def _():
+        s_ref[0] = scores(z, y + 1)
+
+        @pl.loop(y + 1, NY)
+        def _(block):
+            s_ref[1] = scores(z, NY + block)
+            absorb(z, block, s_ref[0])
+            s_ref[0] = scores(z, lax.rem(block + 1, NY))
+            absorb(z, NY + block, s_ref[1])
+
+    pass_values(1)
 
     tail.wait_recv()
     rim = f32(tail_in[8:])
@@ -340,52 +364,54 @@
     summed += taps[1:2] * cpad[7 : 7 + ROWS]
     summed += taps[2:3] * cpad[8 : 8 + ROWS]
     convg[tp] = bf16(ogate[...] * summed)
-    conv.start()
-
-    @pl.loop(y + 1, NY)
-    def _(block):
-        for h in (0, 1):
-            s_ref[h] = scores(z, block * 2 + h)
-        for h in (0, 1):
-            absorb(z, block * 2 + h, s_ref[h])
-
-    pass_values(1)
-
-    @pl.loop(0, NZ - 1)
+    conv.start(0)
+
+    def half_block(source, g):
+        @pl.when((source < z) & (g == 0))
+        def _():
+            s_ref[0] = scores(source, 0)
+
+        @pl.when(source < z)
+        def _():
+            four_tiles(source, g)
+
+    @pl.loop(0, NZ - 2)
     def _(i):
         d, r = i // 2 + 1, lax.rem(i, 2)
         source = lax.rem(z + jnp.where(r == 0, NZ - d, d), NZ)
 
-        @pl.when(source < z)
-        def _():
-            whole_block(source)
-
-        @pl.when((r == 0) & (d < last))
-        def _():
-            pass_keys(d + 1)
-
-        @pl.when(r == 1)
-        def _():
-            pass_values(d + 1)
+        @pl.loop(0, 2)
+        def _(g):
+            @pl.when((g == 1) & (r == 0))
+            def _():
+                pass_keys(d + 1)
+
+            @pl.when((g == 1) & (r == 1))
+            def _():
+                pass_values(d + 1)
+
+            half_block(source, g)
 
         @pl.when(i == 1)
         def _():
-            conv.neighbours_first()
-            conv.neighbours_second()
+            conv.neighbours_first(0)
+            conv.neighbours_second(0)
 
         @pl.when(i == 3)
         def _():
-            conv.opposite(0)
-            conv.opposite(1)
-
-    for tile in range(TILES):
-        stg[y, 0, tile : tile + 1] = m_ref[tile]
-        stg[y, 1, tile : tile + 1] = a_ref[tile, VDIM : VDIM + 1]
-    st_copies = [
-        remote(stg.at[y], stg.at[y], st_send.at[i - 1], st_recv.at[y], at_y(i)) for i in (1, 3, 2)
-    ]
-    for copy in st_copies:
-        copy.start()
+            conv.opposite(0, 1)
+
+    def st_copy(h, i):
+        return remote(stg.at[y, h], stg.at[y, h], st_send.at[h, i - 1], st_recv.at[y, h], at_y(i))
+
+    @pl.loop(0, 2)
+    def _(h):
+        half_block(lax.rem(z + last, NZ), h)
+        for t in range(NY):
+            stg[y, h, t : t + 1] = m_ref[h * NY + t]
+            stg[y, h, NY + t : NY + t + 1] = a_ref[h * NY + t, VDIM : VDIM + 1]
+        for i in (2, 1, 3):
+            st_copy(h, i).start()
 
     for load in loads[6:]:
         load.wait()
@@ -395,72 +421,77 @@
     def mixed(buf, which, slot, rows):
         return jnp.dot(buf[slot, rows], obuf[which, slot], preferred_element_type=jnp.float32)
 
-    oacc[...] = jnp.zeros_like(oacc)
-
-    @pl.loop(0, NTP)
+    oacc[...] = mixed(convg, 1, 0, slice(0, ROWS))
+
+    @pl.loop(1, NTP)
     def _(slot):
         oacc[...] += mixed(convg, 1, slot, slice(0, ROWS))
 
-    for i in (1, 3, 2):
-        peer = lax.rem(y + i, NY)
-        remote(stg.at[peer], stg.at[peer], st_send.at[0], st_recv.at[peer], at_y(1)).wait_recv()
-    m_all = stg[0, 0]
-    for i in range(1, NY):
-        m_all = jnp.maximum(m_all, stg[i, 0])
-    l_all = stg[0, 1] * jnp.exp2(stg[0, 0] - m_all)
-    for i in range(1, NY):
-        l_all = l_all + stg[i, 1] * jnp.exp2(stg[i, 0] - m_all)
-    second = lax.broadcasted_iota(jnp.int32, (TILES, LANES), 1) >= TILE
-    share = jnp.exp2(stg[y, 0] - m_all) / l_all
-    coef[0] = jnp.where(second, -lam[0:1, 0:1] * share, share)
-    coef[1] = m_all * LN2 + jnp.log(l_all)
-
-    def combined(tile):
-        part = a_ref[tile, :VDIM] * coef[0, pl.ds(tile, 1)]
+    to = (at_y(1), at_y(3))
+    near = (lax.rem(y + 1, NY), lax.rem(y + 3, NY))
+    opposite = lax.rem(y + 2, NY)
+    second = lax.broadcasted_iota(jnp.int32, (NY, LANES), 1) >= TILE
+
+    def combined(h, block):
+        part = a_ref[h * NY + block, :VDIM] * coef[h, pl.ds(block, 1)]
         return part[:, :TILE] + part[:, TILE:]
 
-    right, left = lax.rem(y + 1, NY), lax.rem(y + 3, NY)
-    opposite = lax.rem(y + 2, NY)
-    to = (at_y(1), at_y(-1 + NY))
-    near = (right, left)
-    c_copies = []
-
-    def send_part(i, target, device):
-        copy = remote(csend.at[i], target, c_send.at[i], c_recv.at[i], device)
-        copy.start()
-        c_copies.append(copy)
-
-    for w in (0, 1):
-        csend[w] = bf16(combined(opposite * 2 + w))
-    for w in (0, 1):
-        send_part(w, crelay.at[w], to[w])
-    for w in (0, 1):
-        csend[2 + w] = bf16(combined(near[w] * 2 + 1 - w))
-    for w in (0, 1):
-        send_part(2 + w, crecv.at[w, 0], to[w])
-    relayed = [combined(near[w] * 2 + w) for w in (0, 1)]
-    for w in (0, 1):
-        c_copies[w].wait_recv()
-        csend[4 + w] = bf16(relayed[w] + f32(crelay[w]))
-        send_part(4 + w, crecv.at[w, 1], to[w])
-    for h in (0, 1):
+    def part_copy(h, k, target, device):
+        n = 3 * h + k
+        return remote(csend.at[n], target, c_send.at[n], c_recv.at[n], device)
+
+    c_copies = [
+        [
+            part_copy(h, 0, crelay.at[h], to[h]),
+            part_copy(h, 1, crecv.at[h, 0], to[1 - h]),
+            part_copy(h, 2, crecv.at[h, 1], to[h]),
+        ]
+        for h in (0, 1)
+    ]
+
+    def weigh(h):
+        for i in (1, 3, 2):
+            peer = lax.rem(y + i, NY)
+            remote(
+                stg.at[peer, h], stg.at[peer, h], st_send.at[h, 0], st_recv.at[peer, h], at_y(1)
+            ).wait_recv()
+        m_all = stg[0, h, :NY]
+        for i in range(1, NY):
+            m_all = jnp.maximum(m_all, stg[i, h, :NY])
+        l_all = stg[0, h, NY:] * jnp.exp2(stg[0, h, :NY] - m_all)
+        for i in range(1, NY):
+            l_all = l_all + stg[i, h, NY:] * jnp.exp2(stg[i, h, :NY] - m_all)
+        share = jnp.exp2(stg[y, h, :NY] - m_all) / l_all
+        coef[h, :NY] = jnp.where(second, -lam[0] * share, share)
+        coef[h, NY:] = m_all * LN2 + jnp.log(l_all)
+        csend[3 * h] = bf16(combined(h, opposite))
+        c_copies[h][0].start()
+        csend[3 * h + 1] = bf16(combined(h, near[1 - h]))
+        c_copies[h][1].start()
+        cown[:, h * TILE : (h + 1) * TILE] = combined(h, near[h])
+
+    def pass_on(h):
         lanes = slice(h * TILE, (h + 1) * TILE)
-        cown[:, lanes] = combined(y * 2 + h)
-        row = coef[1, pl.ds(y * 2 + h, 1)]
+        c_copies[h][0].wait_recv()
+        csend[3 * h + 2] = bf16(cown[:, lanes] + f32(crelay[h]))
+        c_copies[h][2].start()
+        cown[:, lanes] = combined(h, y)
+        row = coef[h, pl.ds(NY + y, 1)]
         logs[0, 0:1, lanes] = row[:, :TILE]
         logs[0, 1:2, lanes] = row[:, TILE:]
-    for w in (0, 1):
-        c_copies[2 + w].wait_recv()
-        cown[:, (1 - w) * TILE : (2 - w) * TILE] += f32(crecv[w, 0])
-    for w in (0, 1):
-        c_copies[4 + w].wait_recv()
-        cown[:, w * TILE : (w + 1) * TILE] += f32(crecv[w, 1])
-
-    head_mix = cown[...]
-    mean = jnp.sum(head_mix * head_mix, axis=0, keepdims=True) / VDIM
-    normed = jnp.transpose(head_mix * lax.rsqrt(mean + HEAD_EPS))
-    attng[tp] = bf16(normed * head_gain[...] * HEAD_SCALE)
-    attn.start()
+
+    def settle(h):
+        c_copies[h][1].wait_recv()
+        c_copies[h][2].wait_recv()
+        head_mix = cown[:, h * TILE : (h + 1) * TILE] + f32(crecv[h, 0]) + f32(crecv[h, 1])
+        mean = jnp.sum(head_mix * head_mix, axis=0, keepdims=True) / VDIM
+        normed = jnp.transpose(head_mix * lax.rsqrt(mean + HEAD_EPS))
+        attng[tp, h * HALF : (h + 1) * HALF] = bf16(normed * head_gain[...] * HEAD_SCALE)
+        attn.start(2 * h)
+
+    for stage in (weigh, pass_on, settle):
+        for h in (0, 1):
+            stage(h)
 
     def add(slot, h):
         rows = slice(h * HALF, (h + 1) * HALF)
@@ -468,24 +499,7 @@
 
     add(tp, 0)
     add(tp, 1)
-    for h in (0, 1):
-        attn.wait(0, True, h)
-        add(attn.slot(0, True), h)
-    attn.neighbours_first()
-    add(attn.slot(-1, False), 0)
-    add(attn.slot(1, False), 1)
-    attn.neighbours_second()
-    add(attn.slot(-1, False), 1)
-    add(attn.slot(1, False), 0)
-    for dx, h in ((-1, 0), (1, 1), (-1, 1), (1, 0)):
-        attn.wait(dx, True, h)
-        add(attn.slot(dx, True), h)
-    for h in (0, 1):
-        attn.opposite(h)
-        add(attn.slot(2, False), h)
-    for h in (0, 1):
-        attn.wait(2, True, h)
-        add(attn.slot(2, True), h)
+    gathered(attn, add)
     out[...] = bf16(oacc[...])
 
     tokens.finish()
@@ -495,8 +509,11 @@
         if d < NZ // 2 - 1:
             k_copy(z, kd_send.at[d], at_z(-1)).wait_send()
             v_copy(z, vu_send.at[d], at_z(1)).wait_send()
-    for copy in q_copies + st_copies + c_copies + [tail]:
+    for copy in q_copies + c_copies[0] + c_copies[1] + [tail]:
         copy.wait_send()
+    for h in (0, 1):
+        for i in (1, 2, 3):
+            st_copy(h, i).wait_send()
     conv.finish()
     attn.finish()
 
@@ -547,7 +564,7 @@
             pltpu.VMEM((4, 128), fl),
             pltpu.VMEM((2, ROWS, 128), fl),
             pltpu.VMEM((3, VDIM), fl),
-            pltpu.VMEM((1, 128), fl),
+            pltpu.SMEM((1,), fl),
             pltpu.VMEM((1, VDIM), fl),
             pltpu.VMEM((NTP, ROWS, PIECE), bf),
             pltpu.VMEM((NTP, PIECE, 6 * VDIM), bf),
@@ -586,16 +603,16 @@
             dma((NZ,)),
             dma((NY,)),
             dma((NY,)),
-            dma((NY,)),
-            dma((NY,)),
+            dma((2, NY)),
+            dma((NY, 2)),
             dma((6,)),
             dma((6,)),
             dma,
             dma,
             dma((14,)),
             dma((NTP, 2)),
-            dma((14,)),
-            dma((NTP, 2)),
+            dma((28,)),
+            dma((NTP, 4)),
         ],
         compiler_params=pltpu.CompilerParams(
             collective_id=0, has_side_effects=True, vmem_limit_bytes=60 * 2**20
@@ -617,7 +634,7 @@
         jnp.asarray(base),
         jnp.asarray(rows),
         conv_taps,
-        jnp.broadcast_to(lambdas, (1, 128)),
+        lambdas,
         head_gain.reshape(1, VDIM),
         attn_out_weight.reshape(NTP, VDIM, PIECE),
         conv_out_weight.reshape(NTP, VDIM, PIECE),

time: 74.5 us -> 73.3 us (0.984)
  no operation moved by 1% of the time
where the time goes in v3:
time: 73.3 us; the launch traced here: 73.2 us
  Pallas kernels  69.6 us (95%)
  local copies, waits for them, and re-layouts  2.27 us (3%)
  between operations  1.3 us (2%)
    pallas_call x1, Pallas kernels, per_device(): pl.pallas_call(kernel, out_shape=(jax.ShapeDtypeStruct((ROWS, PIECE), bf)...  69.6 us
    unnamed x4, local copies, waits for them, and re-layouts  2.27 us

profile of v3, /device:TPU:225, one launch (start us, length us, event | category | flops | bytes accessed | tf_op | source)
XLA Modules:
  0.0 73.2 jit_solution(2031510119461992952)
XLA Ops:
  1.3 69.6 %shard_map.158 = (bf16[512,256]{1,0:T(8,128)(2,1)}, f32[1,2,512]{2,1,0:T(2,128)}) custom-call(bf16[512,256]{1,0:T(8,128)(2,1)} %tok_in.1, f32[8,1,256]{2,1,0:T(1,128)} %bitcast.18, bf16[8,256,128]{2,1,0:T(8,128)(2,1)} %bitcast.10, bf16[8,256,128]{2,1,0:T(8,128)(2,1)} %bitcast.11, bf16[8,256,128]{2,1,0:T(8,128)(2,1)} %bitcast.12, ...), custom_call_target="tpu_custom_call" | custom-call | tf_op jit(solution)/shard_map/pallas_call | solution.py:553
  70.9 0.0 copy-start
  70.9 1.7 %copy.20 = bf16[512,256]{1,0:T(8,128)(2,1)} copy(bf16[512,256]{1,0:T(8,128)(2,1)} %get-tuple-element.4) | data formatting | bytes 524288
  72.6 0.0 copy-done
  72.6 0.6 copy.21
Async XLA Ops:
  70.9 1.7 %copy-start = (f32[1,2,512]{2,1,0:T(2,128)S(1)}, f32[1,2,512]{2,1,0:T(2,128)}, u32[]{:S(2)}) copy-start(f32[1,2,512]{2,1,0:T(2,128)} %get-tuple-element.5) | copy-start | bytes 12292

commit v4 on v3

--- a/solution.py
+++ b/solution.py
@@ -344,6 +344,8 @@
         remote(qbuf.at[block], qbuf.at[block], q_send.at[0], q_recv.at[block], at_y(1)).wait_recv()
         blocked(block)
 
+    pass_values(1)
+
     @pl.when(y < NY - 1)
     def _():
         s_ref[0] = scores(z, y + 1)
@@ -354,8 +356,6 @@
             absorb(z, block, s_ref[0])
             s_ref[0] = scores(z, lax.rem(block + 1, NY))
             absorb(z, NY + block, s_ref[1])
-
-    pass_values(1)
 
     tail.wait_recv()
     rim = f32(tail_in[8:])
@@ -615,9 +615,9 @@
             dma((NTP, 4)),
         ],
         compiler_params=pltpu.CompilerParams(
-            collective_id=0, has_side_effects=True, vmem_limit_bytes=60 * 2**20
+            collective_id=0, has_side_effects=True, vmem_limit_bytes=40 * 2**20
         ),
-    )(
+    )(*(v if v is lambdas else pltpu.with_memory_space_constraint(v, pltpu.HBM) for v in (
         tokens,
         norm_gain.reshape(NTP, 1, PIECE),
         *(
@@ -638,7 +638,7 @@
         head_gain.reshape(1, VDIM),
         attn_out_weight.reshape(NTP, VDIM, PIECE),
         conv_out_weight.reshape(NTP, VDIM, PIECE),
-    )
+    )))
     return mixed_out, logs
 
 

time: 73.3 us -> 70.3 us (0.959)
  Pallas kernels: 69.6 us -> 67.6 us
  local copies, waits for them, and re-layouts: 2.27 us -> 1.3 us
    pallas_call x1, Pallas kernels: 69.6 us -> 67.6 us  [per_device(): pl.pallas_call(kernel, out_shape=(jax.ShapeDtypeStruct((ROWS, PIECE), bf)...]
    unnamed x4 -> x2, local copies, waits for them, and re-layouts: 2.27 us -> 1.3 us
where the time goes in v4:
time: 70.3 us; the launch traced here: 70.2 us
  Pallas kernels  67.6 us (96%)
  local copies, waits for them, and re-layouts  1.3 us (2%)
  between operations  1.29 us (2%)
    pallas_call x1, Pallas kernels, per_device(): pl.pallas_call(kernel, out_shape=(jax.ShapeDtypeStruct((ROWS, PIECE), bf)...  67.6 us

profile of v4, /device:TPU:225, one launch (start us, length us, event | category | flops | bytes accessed | tf_op | source)
XLA Modules:
  0.0 70.2 jit_solution(8267967414136662138)
XLA Ops:
  1.3 67.6 %shard_map.158 = (bf16[512,256]{1,0:T(8,128)(2,1)S(1)}, f32[1,2,512]{2,1,0:T(2,128)S(1)}) custom-call(bf16[512,256]{1,0:T(8,128)(2,1)} %tok_in.1, f32[8,1,256]{2,1,0:T(1,128)} %bitcast.18, bf16[8,256,128]{2,1,0:T(8,128)(2,1)} %bitcast.10, bf16[8,256,128]{2,1,0:T(8,128)(2,1)} %bitcast.11, bf16[8,256,128]{2,1,0:T(8,128)(2,1)} %bitcast.12, ...), custom_call_target="tpu_custom_call" | custom-call | tf_op jit(solution)/shard_map/pallas_call | solution.py:553
  68.9 0.7 %copy.20 = bf16[512,256]{1,0:T(8,128)(2,1)} copy(bf16[512,256]{1,0:T(8,128)(2,1)S(1)} %get-tuple-element.4) | data formatting | bytes 524288
  69.6 0.6 copy.21

commit v5 on v4

--- a/solution.py
+++ b/solution.py
@@ -296,10 +296,12 @@
         )
 
     def four_tiles(slot, g):
-        for i in range(4):
-            tile = g * 4 + i
-            s_ref[(i + 1) % 2] = scores(slot, lax.rem(tile + 1, TILES))
-            absorb(slot, tile, s_ref[i % 2])
+        if g == 0:
+            s_ref[0] = scores(slot, 0)
+        for tile in range(4 * g, 4 * g + 4):
+            if tile + 1 < TILES:
+                s_ref[(tile + 1) % 2] = scores(slot, tile + 1)
+            absorb(slot, tile, s_ref[tile % 2])
 
     blocked(y)
     for h in (0, 1):
@@ -367,10 +369,6 @@
     conv.start(0)
 
     def half_block(source, g):
-        @pl.when((source < z) & (g == 0))
-        def _():
-            s_ref[0] = scores(source, 0)
-
         @pl.when(source < z)
         def _():
             four_tiles(source, g)
@@ -380,17 +378,17 @@
         d, r = i // 2 + 1, lax.rem(i, 2)
         source = lax.rem(z + jnp.where(r == 0, NZ - d, d), NZ)
 
-        @pl.loop(0, 2)
-        def _(g):
-            @pl.when((g == 1) & (r == 0))
-            def _():
-                pass_keys(d + 1)
-
-            @pl.when((g == 1) & (r == 1))
-            def _():
-                pass_values(d + 1)
-
-            half_block(source, g)
+        half_block(source, 0)
+
+        @pl.when(r == 0)
+        def _():
+            pass_keys(d + 1)
+
+        @pl.when(r == 1)
+        def _():
+            pass_values(d + 1)
+
+        half_block(source, 1)
 
         @pl.when(i == 1)
         def _():
@@ -404,8 +402,7 @@
     def st_copy(h, i):
         return remote(stg.at[y, h], stg.at[y, h], st_send.at[h, i - 1], st_recv.at[y, h], at_y(i))
 
-    @pl.loop(0, 2)
-    def _(h):
+    for h in (0, 1):
         half_block(lax.rem(z + last, NZ), h)
         for t in range(NY):
             stg[y, h, t : t + 1] = m_ref[h * NY + t]

time: 70.3 us -> 69.7 us (level)
  no operation moved by 1% of the time
where the time goes in v5:
time: 69.7 us; the launch traced here: 69.6 us
  Pallas kernels  67 us (96%)
  local copies, waits for them, and re-layouts  1.3 us (2%)
  between operations  1.29 us (2%)
    pallas_call x1, Pallas kernels, per_device(): pl.pallas_call(kernel, out_shape=(jax.ShapeDtypeStruct((ROWS, PIECE), bf)...  67 us

profile of v5, /device:TPU:225, one launch (start us, length us, event | category | flops | bytes accessed | tf_op | source)
XLA Modules:
  0.0 69.6 jit_solution(12473269930319988900)
XLA Ops:
  1.3 67.0 %shard_map.158 = (bf16[512,256]{1,0:T(8,128)(2,1)S(1)}, f32[1,2,512]{2,1,0:T(2,128)S(1)}) custom-call(bf16[512,256]{1,0:T(8,128)(2,1)} %tok_in.1, f32[8,1,256]{2,1,0:T(1,128)} %bitcast.18, bf16[8,256,128]{2,1,0:T(8,128)(2,1)} %bitcast.10, bf16[8,256,128]{2,1,0:T(8,128)(2,1)} %bitcast.11, bf16[8,256,128]{2,1,0:T(8,128)(2,1)} %bitcast.12, ...), custom_call_target="tpu_custom_call" | custom-call | tf_op jit(solution)/shard_map/pallas_call | solution.py:550
  68.3 0.7 %copy.20 = bf16[512,256]{1,0:T(8,128)(2,1)} copy(bf16[512,256]{1,0:T(8,128)(2,1)S(1)} %get-tuple-element.4) | data formatting | bytes 524288
  69.0 0.6 copy.21
